TPU v7x, 256 devices: a whole 4x4x8 slice. The times are simulated.
256 devices in a mesh: sp: 32 (over z, x), tp: 8 (over y, core).
Axes of the slice: x: 4, y: 4, z: 8, core: 2. Of those that a mesh axis runs over, the one named last changes fastest.
Arguments:
- tokens: bfloat16 [32768, 2048], P('sp', 'tp'), may hold values from -6 to 6
- norm_gain: float32 [2048], replicated, may hold values from 0.1 to 1.9
- att_query: bfloat16 [2048, 1024], P(None, 'tp'), may hold values from -1 to 1
- att_key: bfloat16 [2048, 512], P(None, 'tp'), may hold values from -16 to 16
- att_value: bfloat16 [2048, 512], P(None, 'tp'), may hold values from -0.125 to 0.125
- ret_query: bfloat16 [2048, 512], P(None, 'tp'), may hold values from -0.125 to 0.125
- ret_key: bfloat16 [2048, 512], P(None, 'tp'), may hold values from -0.125 to 0.125
- ret_value: bfloat16 [2048, 1024], P(None, 'tp'), may hold values from -0.125 to 0.125
- ret_gate: bfloat16 [2048, 1024], P(None, 'tp'), may hold values from -0.125 to 0.125
- att_sink: float32 [16], P('tp'), may hold values from 4 to 7
- decay_log: float32 [8, 32768], P('tp', 'sp'), may hold values from -2 to 0, as said below
- init_state: float32 [2, 8, 64, 128], P(None, 'tp'), may hold values from -24 to 24
- out_att: bfloat16 [1024, 2048], P('tp'), may hold values from -0.125 to 0.125
- out_ret: bfloat16 [1024, 2048], P('tp'), may hold values from -0.125 to 0.125
Outputs:
- mixed: bfloat16 [32768, 2048], P('sp', 'tp')
Inputs may be any that keep to these rules, and one draw needn't show every extreme that they name: `decay_log`: log decays, negative.
All inputs are finite; a program needn't handle non-finite values.
Results may differ from a plain program's by a relative error of at most 0.02.
Values may be sent and summed in bfloat16 or wider, within the bound.
A program may use at most 64 MiB of HBM per device.

v0:
```python
import jax
import jax.numpy as jnp
from jax import lax
from jax.sharding import PartitionSpec as P

HD = 64
RK = 64
RV = 128
WINDOW = 128
RET_BLOCK = 128


NORM_EPS = 1e-06
ROPE_BASE = 10000.0


def padded_2(block, sides, width):
    for axis, dim in sides:
        count = lax.axis_size(axis)
        forward = [(i, i + 1) for i in range(count - 1)]
        backward = [(target, source) for source, target in forward]
        low = lax.ppermute(
            lax.slice_in_dim(block, block.shape[dim] - width, None, axis=dim), axis, forward
        )
        high = lax.ppermute(lax.slice_in_dim(block, 0, width, axis=dim), axis, backward)
        block = jnp.concatenate([low, block, high], axis=dim)
    return block


def copy_for_each(value, axis):
    copies = jnp.broadcast_to(value, (lax.axis_size(axis), *value.shape))
    return lax.all_to_all(copies, axis, split_axis=0, concat_axis=0, tiled=True)


def all_in_one(value, axis):
    leaves = jax.tree.leaves(value)
    sequence = sorted(range(len(leaves)), key=lambda k: -leaves[k].size)
    width = (1, *leaves[sequence[0]].shape)[-1]
    lines = [
        jnp.pad(leaves[k].reshape(-1), (0, -leaves[k].size % width)).reshape(-1, width)
        for k in sequence
    ]
    both, at, found = (copy_for_each(jnp.concatenate(lines), axis), 0, {})
    for k, line in zip(sequence, lines):
        piece = both[:, at : at + len(line)].reshape(len(both), -1)
        found[k] = piece[:, : leaves[k].size].reshape(-1, *leaves[k].shape)
        at += len(line)
    numbers = iter(range(len(leaves)))
    return jax.tree.map(lambda _: found[next(numbers)], value)


def combined_pairwise(pieces, combine):
    while len(jax.tree.leaves(pieces)[0]) > 1:
        pieces = jax.vmap(combine)(
            *(jax.tree.map(lambda part: part[side::2], pieces) for side in (0, 1))
        )
    return jax.tree.map(lambda part: part[0], pieces)


def carried_in(value, axis, combine, identity, reverse):
    length, index = (lax.axis_size(axis), lax.axis_index(axis))
    passed = jnp.arange(length) > index if reverse else jnp.arange(length) < index

    def kept(part, zero, own):
        part = jnp.where(
            passed.reshape(-1, *(1 for _ in own.shape)),
            part.astype(own.dtype),
            jnp.asarray(zero, own.dtype),
        )
        return part[::-1] if reverse else part

    pieces = all_in_one(
        jax.tree.map(lambda part, kind: part.astype(kind), value, (jnp.bfloat16, jnp.bfloat16)),
        axis,
    )
    return combined_pairwise(jax.tree.map(kept, pieces, identity, value), combine)


def rotated(values, positions):
    half_dim = values.shape[-1] // 2
    inverse = ROPE_BASE ** (-2.0 * jnp.arange(half_dim, dtype=jnp.float32) / values.shape[-1])
    angles = positions.astype(jnp.float32)[:, None] * inverse[None, :]
    cosine = jnp.cos(angles)[:, None, :]
    sine = jnp.sin(angles)[:, None, :]
    first_half = values[..., :half_dim]
    second_half = values[..., half_dim:]
    return jnp.concatenate(
        [first_half * cosine - second_half * sine, first_half * sine + second_half * cosine],
        axis=-1,
    )


def advance(state_now, item_pair):
    factor_now, term_now = item_pair
    return (factor_now[:, None, None] * state_now + term_now, state_now)


def compose(earlier, later_map):
    return (earlier[0] * later_map[0], later_map[0][:, None, None] * earlier[1] + later_map[1])


def body(
    tokens,
    norm_gain,
    att_query,
    att_key,
    att_value,
    ret_query,
    ret_key,
    ret_value,
    ret_gate,
    att_sink,
    decay_log,
    init_state,
    out_att,
    out_ret,
):
    tok_rows = tokens.shape[0]
    chan_local = tokens.shape[1]
    query_cols = att_query.shape[1]
    kv_cols = att_key.shape[1]
    rk_cols = ret_query.shape[1]
    rv_cols = ret_value.shape[1]
    heads_local = att_sink.shape[0]
    kv_local = kv_cols // HD
    groups = heads_local // kv_local
    ret_local = decay_log.shape[0]
    seq_offset = lax.axis_index("sp") * tok_rows
    seq_len = tok_rows * lax.axis_size("sp")
    joined = jnp.concatenate(
        [att_query, att_key, att_value, ret_query, ret_key, ret_value, ret_gate], axis=1
    )
    piece_f = lax.all_gather(tokens, "tp", axis=1, tiled=True).astype(jnp.float32)
    scaled = (piece_f * norm_gain[None, :]).astype(jnp.bfloat16)
    proj_sums = jnp.dot(scaled, joined, preferred_element_type=jnp.float32)
    squares = jnp.sum(piece_f * piece_f, axis=1)
    inv_rms = lax.rsqrt(squares / (chan_local * lax.axis_size("tp")) + NORM_EPS)
    projected = (proj_sums * inv_rms[:, None]).astype(jnp.bfloat16)
    off_rq = query_cols + 2 * kv_cols
    off_rk = off_rq + rk_cols
    off_rv = off_rk + rk_cols
    off_gate = off_rv + rv_cols
    key_vals = projected[:, query_cols:off_rq]
    padded = padded_2(key_vals, (("sp", 0),), WINDOW)
    block_rows = min(512, tok_rows)
    span_rows = block_rows + 2 * WINDOW
    queries = projected[:, :query_cols].reshape(tok_rows, kv_local, groups, HD)
    sink_col = att_sink.reshape(kv_local, groups, 1, 1)
    outputs = []
    for first_row in range(0, tok_rows, block_rows):
        query_block = queries[first_row : first_row + block_rows]
        span_block = padded[first_row : first_row + span_rows]
        key_block = span_block[:, :kv_cols].reshape(span_rows, kv_local, HD)
        value_block = span_block[:, kv_cols:].reshape(span_rows, kv_local, HD)
        scores = jnp.einsum(
            "qkgd,skd->kgqs", query_block, key_block, preferred_element_type=jnp.float32
        ) * HD ** (-0.5)
        query_pos = seq_offset + first_row + jnp.arange(block_rows, dtype=jnp.int32)
        key_pos = seq_offset + first_row - WINDOW + jnp.arange(span_rows, dtype=jnp.int32)
        allowed = (
            (jnp.abs(query_pos[:, None] - key_pos[None, :]) <= WINDOW)
            & (key_pos >= 0)[None, :]
            & (key_pos < seq_len)[None, :]
        )
        scores = jnp.where(allowed, scores, -jnp.inf)
        row_top = jnp.maximum(jnp.max(scores, axis=-1, keepdims=True), sink_col)
        raised = jnp.exp(scores - row_top)
        denominator = jnp.sum(raised, axis=-1, keepdims=True) + jnp.exp(sink_col - row_top)
        weights_bf = (raised / denominator).astype(jnp.bfloat16)
        block_out = jnp.einsum(
            "kgqs,skd->qkgd", weights_bf, value_block, preferred_element_type=jnp.float32
        )
        outputs.append(block_out.reshape(block_rows, query_cols).astype(jnp.bfloat16))
    attended = jnp.concatenate(outputs, axis=0)
    positions = seq_offset + jnp.arange(tok_rows, dtype=jnp.int32)
    query_rot = rotated(
        projected[:, off_rq:off_rk].astype(jnp.float32).reshape(tok_rows, ret_local, RK), positions
    )
    key_rot = rotated(
        projected[:, off_rk:off_rv].astype(jnp.float32).reshape(tok_rows, ret_local, RK), positions
    ) * RK ** (-0.5)
    value_f = projected[:, off_rv:off_gate].astype(jnp.float32).reshape(tok_rows, ret_local, RV)
    gate_f = projected[:, off_gate:].astype(jnp.float32)
    block_count = tok_rows // RET_BLOCK

    def heads_first(values, width):
        return jnp.transpose(values.reshape(block_count, RET_BLOCK, ret_local, width), (2, 0, 1, 3))

    query_h = heads_first(query_rot, RK)
    key_h = heads_first(key_rot, RK)
    value_h = heads_first(value_f, RV)
    block_logs = decay_log.reshape(ret_local, block_count, RET_BLOCK)
    cumul = jnp.cumsum(block_logs, axis=-1)
    block_log = cumul[..., -1]
    inner_w = jnp.einsum("hbnk,hbmk->hbnm", query_h, key_h) * jnp.exp(
        -jnp.abs(cumul[..., :, None] - cumul[..., None, :])
    )
    local_out = jnp.einsum("hbnm,hbmv->hbnv", inner_w, value_h)
    fwd_terms = jnp.einsum(
        "hbmk,hbmv->bhkv", key_h * jnp.exp(block_log[..., None] - cumul)[..., None], value_h
    )
    bwd_terms = jnp.einsum("hbmk,hbmv->bhkv", key_h * jnp.exp(cumul)[..., None], value_h)
    factors = jnp.exp(block_log).T
    zero_state = jnp.zeros((ret_local, RK, RV), jnp.float32)
    fwd_total, fwd_local = lax.scan(advance, zero_state, (factors, fwd_terms))
    bwd_total, bwd_local = lax.scan(advance, zero_state, (factors, bwd_terms), reverse=True)
    before_log = jnp.cumsum(block_log, axis=1) - block_log
    after_log = jnp.sum(block_log, axis=1, keepdims=True) - jnp.cumsum(block_log, axis=1)
    device_factor = jnp.exp(jnp.sum(block_log, axis=1))
    identity_map = (jnp.ones((ret_local,), jnp.float32), zero_state)
    fwd_factor, fwd_sum = carried_in((device_factor, fwd_total), "sp", compose, identity_map, False)
    bwd_factor, bwd_sum = carried_in((device_factor, bwd_total), "sp", compose, identity_map, True)
    fwd_start = fwd_factor[:, None, None] * init_state[0] + fwd_sum
    bwd_start = bwd_factor[:, None, None] * init_state[1] + bwd_sum
    fwd_in = fwd_local + jnp.exp(before_log).T[:, :, None, None] * fwd_start[None]
    bwd_in = bwd_local + jnp.exp(after_log).T[:, :, None, None] * bwd_start[None]
    cross_out = jnp.exp(cumul)[..., None] * jnp.einsum("hbnk,bhkv->hbnv", query_h, fwd_in)
    cross_out = cross_out + jnp.exp(block_log[..., None] - cumul)[..., None] * jnp.einsum(
        "hbnk,bhkv->hbnv", query_h, bwd_in
    )
    combined = local_out + cross_out
    centered = combined - jnp.mean(combined, axis=-1, keepdims=True)
    normed = centered * lax.rsqrt(jnp.mean(centered * centered, axis=-1, keepdims=True) + NORM_EPS)
    retained = jnp.transpose(normed, (1, 2, 0, 3)).reshape(tok_rows, ret_local * RV)
    ret_out = (jax.nn.silu(gate_f) * retained).astype(jnp.bfloat16)
    contract_dims = (((0,), (1,)), ((), ()))
    att_part = lax.dot_general(out_att, attended, contract_dims, preferred_element_type=jnp.float32)
    summed = lax.psum_scatter(
        (
            att_part
            + lax.dot_general(out_ret, ret_out, contract_dims, preferred_element_type=jnp.float32)
        ).astype(jnp.bfloat16),
        "tp",
        scatter_dimension=0,
        tiled=True,
    ).astype(jnp.float32)
    return summed.T.astype(jnp.bfloat16)


def solution(mesh):
    in_specs = (
        P("sp", "tp"),
        P(),
        P(None, "tp"),
        P(None, "tp"),
        P(None, "tp"),
        P(None, "tp"),
        P(None, "tp"),
        P(None, "tp"),
        P(None, "tp"),
        P("tp"),
        P("tp", "sp"),
        P(None, "tp", None, None),
        P("tp", None),
        P("tp", None),
    )
    out_specs = P("sp", "tp")
    return jax.shard_map(body, mesh=mesh, in_specs=in_specs, out_specs=out_specs, check_vma=False)
```

profile of v0, /device:TPU:1, one launch (start us, length us, event | category | flops | bytes accessed | tf_op | source)
XLA Modules:
  0.0 196.2 jit_solution(13642137882907358056)
XLA Ops:
  6.5 0.7 all-gather.2.cloned.1.call-update
  7.3 1.0 reduce_window_sum.19
  8.3 0.7 slice_reduce_fusion
  9.7 2.0 copy.53
  11.6 2.0 copy.54
  13.6 2.0 %copy.55 = bf16[2048,64]{1,0:T(8,128)(2,1)} copy(bf16[2048,64]{0,1:T(8,128)(2,1)} %param.23) | data formatting | bytes 524288 | tf_op args[5]
  15.5 2.0 %copy.56 = bf16[2048,64]{1,0:T(8,128)(2,1)} copy(bf16[2048,64]{0,1:T(8,128)(2,1)} %param.24) | data formatting | bytes 524288 | tf_op args[6]
  17.7 5.5 %concatenate.39 = bf16[2048,640]{1,0:T(8,128)(2,1)S(1)} concatenate(bf16[2048,128]{1,0:T(8,128)(2,1)} %param.20, bf16[2048,64]{1,0:T(8,128)(2,1)} %copy.53, bf16[2048,64]{1,0:T(8,128)(2,1)} %copy.54, bf16[2048,64]{1,0:T(8,128)(2,1)} %copy.55, bf16[2048,64]{1,0:T(8,128)(2,1)} %copy.56, bf16[2048,128]{1,0:T(8,128)(2,1)} %param.25, bf16[2048,128]{1,0:T(8,128)(2,1)} %param.26), dimensions={1} | concatenate | bytes 5242880 | tf_op jit(solution)/shard_map/concatenate | solution.py:130
  23.3 0.6 fusion.106
  24.0 1.4 fusion.17
  25.4 1.4 fusion.19
  26.9 24.7 %all-gather.2.cloned.1.call-done = bf16[1024,2048]{1,0:T(8,128)(2,1)} async-done(((bf16[1024,256]{1,0:T(8,128)(2,1)}), bf16[1024,2048]{1,0:T(8,128)(2,1)}) %all-gather.2.cloned.1.call-update) | async-done | bytes 4194320 | tf_op jit(solution)/shard_map/all_gather | solution.py:133
  51.5 3.2 %fusion.1 = f32[1024]{0:T(1024)S(1)} fusion(bf16[1024,2048]{1,0:T(8,128)(2,1)} %all-gather.2.cloned.1.call-done), kind=kLoop, calls=%fused_computation.9 | loop fusion | flops 6290432 | bytes 4198400 | tf_op jit(solution)/shard_map/reduce_sum | solution.py:136
  55.0 3.0 %multiply_convert_fusion = bf16[1024,640]{0,1:T(8,128)(2,1)S(1)} fusion(bf16[2048,640]{1,0:T(8,128)(2,1)S(1)} %concatenate.39, bf16[1024,2048]{1,0:T(8,128)(2,1)S(1)} %copy-done.1, f32[2048]{0:T(1024)S(1)} %copy-done.14, f32[1024]{0:T(1024)S(1)} %add_rsqrt_fusion.1), kind=kOutput, calls=%fused_computation.22 | convolution fusion | flops 2691956736 | bytes 8138752 | tf_op jit(solution)/shard_map/dot_general | solution.py:135
  58.1 3.1 %collective-permute-start = (bf16[128,128]{0,1:T(8,128)(2,1)S(1)}, bf16[128,128]{0,1:T(8,128)(2,1)S(1)}, u32[]{:S(2)}, u32[]{:S(2)}) collective-permute-start(bf16[128,128]{0,1:T(8,128)(2,1)S(1)} %get-tuple-element.235), channel_id=1, source_target_pairs={{0,8},{8,16},{16,24},{24,32},{32,40},{40,48},{48,56},{56,64},{64,7... | collective-permute-start | bytes 98312 | tf_op jit(solution)/shard_map/ppermute | solution.py:22
  61.2 1.3 collective-permute-start.1
  64.2 9.5 %while.31 = (s32[]{:T(128)}, f32[1,64,128]{2,1,0:T(8,128)S(1)}, f32[8,1,64,128]{3,2,1,0:T(8,128)S(1)}, f32[8,1]{0,1:T(1,128)S(1)}, f32[8,1,64,128]{3,2,1,0:T(8,128)S(1)}, /*index=5*/s32[]{:T(128)}, s32[]{:T(128)}, s32[]{:T(128)}) while((s32[]{:T(128)}, f32[1,64,128]{2,1,0:T(8,128)S(1)}, f32[8,1,64,128]{3,2,1,0:T(8,128)S(1)}, ...), condition=%wide.region_11.12_spmd.clone, body=%wide.region_10.11_spmd.clone.sunk | while | flops 32772 | bytes 163980 | solution.py:206
  64.2 0.6 constant_dynamic-slice_fusion.5
  65.4 0.6 constant_dynamic-slice_fusion.5
  66.6 0.6 constant_dynamic-slice_fusion.5
  67.8 0.6 constant_dynamic-slice_fusion.5
  70.1 0.6 constant_dynamic-slice_fusion.5
  71.3 0.6 constant_dynamic-slice_fusion.5
  72.5 0.6 constant_dynamic-slice_fusion.5
  73.7 0.7 copy-done.8
  74.6 9.5 %while.30 = (s32[]{:T(128)}, f32[1,64,128]{2,1,0:T(8,128)S(1)}, f32[8,1,64,128]{3,2,1,0:T(8,128)S(1)}, f32[8,1]{0,1:T(1,128)S(1)}, f32[8,1,64,128]{3,2,1,0:T(8,128)S(1)}, /*index=5*/s32[]{:T(128)}, s32[]{:T(128)}) while((s32[]{:T(128)}, f32[1,64,128]{2,1,0:T(8,128)S(1)}, f32[8,1,64,128]{3,2,1,0:T(8,128)S(1)}, ...), condition=%wide.region_7.8_spmd.clone, body=%wide.region_6.7_spmd.clone.sunk | while | flops 32771 | bytes 163960 | solution.py:205
  74.6 0.6 constant_dynamic-slice_fusion.4
  75.8 0.6 constant_dynamic-slice_fusion.4
  77.0 0.6 constant_dynamic-slice_fusion.4
  81.7 0.6 constant_dynamic-slice_fusion.4
  84.1 0.9 broadcast_in_dim.64
  85.0 11.5 %all-to-all-start.1 = ((bf16[32,65,128]{2,1,0:T(8,128)(2,1)}), bf16[32,65,128]{2,1,0:T(8,128)(2,1)S(1)}, u32[]{:S(2)}, u32[]{:S(2)}) async-start(bf16[32,65,128]{2,1,0:T(8,128)(2,1)} %broadcast_in_dim.64), calls=%async_computation.1 | async-start | bytes 1179648 | tf_op jit(solution)/shard_map/all_to_all | solution.py:32
  97.0 1.0 fusion.121
  98.0 0.8 fusion.8
  98.9 0.8 fusion.6
  99.6 0.8 fusion.9
  100.5 1.6 copy-done.2
  102.1 0.8 fusion.7
  102.9 1.1 fusion.23
  104.0 9.6 %all-to-all-done.1 = bf16[32,65,128]{2,1,0:T(8,128)(2,1)S(1)} async-done(((bf16[32,65,128]{2,1,0:T(8,128)(2,1)}), bf16[32,65,128]{2,1,0:T(8,128)(2,1)S(1)}, u32[]{:S(2)}, u32[]{:S(2)}) %all-to-all-start.1) | async-done | bytes 532512 | tf_op jit(solution)/shard_map/all_to_all | solution.py:32
  113.7 0.9 broadcast_in_dim.60
  114.6 5.5 %all-to-all-start = ((bf16[32,65,128]{2,1,0:T(8,128)(2,1)}), bf16[32,65,128]{2,1,0:T(8,128)(2,1)S(1)}, u32[]{:S(2)}, u32[]{:S(2)}) async-start(bf16[32,65,128]{2,1,0:T(8,128)(2,1)} %broadcast_in_dim.60), calls=%async_computation | async-start | bytes 1179648 | tf_op jit(solution)/shard_map/all_to_all | solution.py:32
  120.2 3.0 %fusion.26 = bf16[64,2,512]{2,0,1:T(8,128)(2,1)S(1)} fusion(f32[2,512]{1,0:T(2,128)S(1)} %exponential_add_fusion, f32[2,512]{1,0:T(2,128)S(1)} %get-tuple-element.274, f32[768,512,2]{1,0,2:T(8,128)} %copy-done.2, pred[512,768]{0,1:T(8,128)(4,1)S(1)} %copy-done.3, bf16[128,128]{0,1:T(8,128)(2,1)S(1)} %collective-permute-done.1, bf16[1024,128]{0,1:T(8,128)(2,1)} %copy-done.11), kind=kOutput, calls=%fused_computation.44 | convolution fusion | flops 104857600 | bytes 3973120 | tf_op jit(solution)/shard_map/kgqs,skd->qkgd/dot_general | solution.py:170
  123.2 4.5 %fusion.40 = f32[1024,2048]{1,0:T(8,128)} fusion(bf16[128,2048]{1,0:T(8,128)(2,1)S(1)} %copy-done, bf16[512,128]{0,1:T(8,128)(2,1)S(1)} %bitcast.200, bf16[512,128]{0,1:T(8,128)(2,1)S(1)} %bitcast.199), kind=kOutput, calls=%fused_computation.63 | convolution fusion | flops 537395200 | bytes 9175040 | tf_op jit(solution)/shard_map/dot_general | solution.py:227
  127.7 9.0 %all-to-all-done = bf16[32,65,128]{2,1,0:T(8,128)(2,1)S(1)} async-done(((bf16[32,65,128]{2,1,0:T(8,128)(2,1)}), bf16[32,65,128]{2,1,0:T(8,128)(2,1)S(1)}, u32[]{:S(2)}, u32[]{:S(2)}) %all-to-all-start) | async-done | bytes 532512 | tf_op jit(solution)/shard_map/all_to_all | solution.py:32
  142.8 1.3 fusion.98
  145.9 6.8 %fusion.5 = bf16[2048,1024]{0,1:T(8,128)(2,1)} fusion(f32[1024,2048]{1,0:T(8,128)} %fusion.40, bf16[128,2048]{1,0:T(8,128)(2,1)S(1)} %copy-done.10, f32[1024,128]{0,1:T(8,128)S(1)} %copy.76, bf16[1024,640]{0,1:T(8,128)(2,1)} %copy-done.5), kind=kOutput, calls=%fused_computation.13 | convolution fusion | flops 541982720 | bytes 13893632 | tf_op jit(solution)/shard_map/dot_general | solution.py:231
  152.7 36.6 %reduce-scatter.2.cloned.1.call-done = bf16[256,1024]{0,1:T(8,128)(2,1)} async-done(((bf16[2048,1024]{0,1:T(8,128)(2,1)}), bf16[256,1024]{0,1:T(8,128)(2,1)}) %reduce-scatter.2.cloned.1.call-update) | async-done | bytes 524304 | tf_op jit(solution)/shard_map/reduce_scatter | solution.py:228
  (161 shorter events, 20.6 us)
Async XLA Ops:
  6.5 116.7 %copy-start = (bf16[128,2048]{1,0:T(8,128)(2,1)S(1)}, bf16[128,2048]{1,0:T(8,128)(2,1)}, u32[]{:S(2)}) copy-start(bf16[128,2048]{1,0:T(8,128)(2,1)} %param.30) | copy-start | bytes 1572868
  6.5 45.0 %all-gather.2.cloned.1.call-start = ((), (), s32[]{:S(2)}) async-start(), calls=%async_computation.3 | async-start | bytes 4718592 | tf_op jit(solution)/shard_map/all_gather | solution.py:133
  23.1 31.6 %copy-start.14 = (f32[2048]{0:T(1024)S(1)}, f32[2048]{0:T(1024)}, u32[]{:S(2)}) copy-start(f32[2048]{0:T(1024)} %param.19) | copy-start | bytes 24580
  51.5 3.4 %copy-start.1 = (bf16[1024,2048]{1,0:T(8,128)(2,1)S(1)}, bf16[1024,2048]{1,0:T(8,128)(2,1)}, u32[]{:S(2)}) copy-start(bf16[1024,2048]{1,0:T(8,128)(2,1)} %all-gather.2.cloned.1.call-done) | copy-start | bytes 12582916
  57.9 4.5 %copy-start.5 = (bf16[1024,640]{0,1:T(8,128)(2,1)}, bf16[1024,640]{0,1:T(8,128)(2,1)S(1)}, u32[]{:S(2)}) copy-start(bf16[1024,640]{0,1:T(8,128)(2,1)S(1)} %multiply_convert_fusion) | copy-start | bytes 3932164
  58.0 44.9 %copy-start.11 = (bf16[1024,128]{0,1:T(8,128)(2,1)}, bf16[1024,128]{0,1:T(8,128)(2,1)S(1)}, u32[]{:S(2)}) copy-start(bf16[1024,128]{0,1:T(8,128)(2,1)S(1)} %get-tuple-element.234) | copy-start | bytes 786436
  58.1 39.9 %collective-permute-start = (bf16[128,128]{0,1:T(8,128)(2,1)S(1)}, bf16[128,128]{0,1:T(8,128)(2,1)S(1)}, u32[]{:S(2)}, u32[]{:S(2)}) collective-permute-start(bf16[128,128]{0,1:T(8,128)(2,1)S(1)} %get-tuple-element.235), channel_id=1, source_target_pairs={{0,8},{8,16},{16,24},{24,32},{32,40},{40,48},{48,56},{56,64},{64,7... | collective-permute-start | bytes 98312 | tf_op jit(solution)/shard_map/ppermute | solution.py:22
  61.2 38.5 %collective-permute-start.1 = (bf16[128,128]{0,1:T(8,128)(2,1)S(1)}, bf16[128,128]{0,1:T(8,128)(2,1)S(1)}, u32[]{:S(2)}, u32[]{:S(2)}) collective-permute-start(bf16[128,128]{0,1:T(8,128)(2,1)S(1)} %get-tuple-element.236), channel_id=1, source_target_pairs={{8,0},{16,8},{24,16},{32,24},{40,32},{48,40},{56,48},{64,56},{72,6... | collective-permute-start | bytes 98312 | tf_op jit(solution)/shard_map/ppermute | solution.py:25
  64.2 33.8 %copy-start.4 = (pred[512,768]{0,1:T(8,128)(4,1)S(1)}, pred[512,768]{0,1:T(8,128)(4,1)}, u32[]{:S(2)}) copy-start(pred[512,768]{0,1:T(8,128)(4,1)} %fusion.17) | copy-start | bytes 1179652
  73.7 0.7 copy-start.8
  84.1 12.5 %copy-start.6 = (f32[8,1,64,128]{3,2,1,0:T(8,128)}, f32[8,1,64,128]{3,2,1,0:T(8,128)S(1)}, u32[]{:S(2)}) copy-start(f32[8,1,64,128]{3,2,1,0:T(8,128)S(1)} %get-tuple-element.137) | copy-start | bytes 786436
  85.0 28.7 %all-to-all-start.1 = ((bf16[32,65,128]{2,1,0:T(8,128)(2,1)}), bf16[32,65,128]{2,1,0:T(8,128)(2,1)S(1)}, u32[]{:S(2)}, u32[]{:S(2)}) async-start(bf16[32,65,128]{2,1,0:T(8,128)(2,1)} %broadcast_in_dim.64), calls=%async_computation.1 | async-start | bytes 1179648 | tf_op jit(solution)/shard_map/all_to_all | solution.py:32
  96.5 2.3 %copy-start.13 = (f32[2]{0:T(128)S(1)}, f32[2]{0:T(128)}, u32[]{:S(2)}) copy-start(f32[2]{0:T(128)} %param.27) | copy-start | bytes 28
  98.0 1.7 copy-start.3
  100.4 1.7 copy-start.2
  114.6 22.1 %all-to-all-start = ((bf16[32,65,128]{2,1,0:T(8,128)(2,1)}), bf16[32,65,128]{2,1,0:T(8,128)(2,1)S(1)}, u32[]{:S(2)}, u32[]{:S(2)}) async-start(bf16[32,65,128]{2,1,0:T(8,128)(2,1)} %broadcast_in_dim.60), calls=%async_computation | async-start | bytes 1179648 | tf_op jit(solution)/shard_map/all_to_all | solution.py:32
  120.2 69.2 %reduce-scatter.2.cloned.1.call-start = ((), (), s32[]{:S(2)}) async-start(), calls=%async_computation.4 | async-start | bytes 4718592 | tf_op jit(solution)/shard_map/reduce_scatter | solution.py:228
  139.5 3.3 %copy-start.12 = (f32[2,1,64,128]{3,2,1,0:T(8,128)S(1)}, f32[2,1,64,128]{3,2,1,0:T(8,128)}, u32[]{:S(2)}) copy-start(f32[2,1,64,128]{3,2,1,0:T(8,128)} %param.29) | copy-start | bytes 196612
  139.5 4.6 %copy-start.7 = (f32[8,1,64,128]{3,2,1,0:T(8,128)S(1)}, f32[8,1,64,128]{3,2,1,0:T(8,128)}, u32[]{:S(2)}) copy-start(f32[8,1,64,128]{3,2,1,0:T(8,128)} %copy-done.6) | copy-start | bytes 786436
  139.6 4.8 %copy-start.9 = (f32[8,1,64,128]{3,2,1,0:T(8,128)S(1)}, f32[8,1,64,128]{3,2,1,0:T(8,128)}, u32[]{:S(2)}) copy-start(f32[8,1,64,128]{3,2,1,0:T(8,128)} %copy-done.8) | copy-start | bytes 786436
  142.7 3.2 %copy-start.10 = (bf16[128,2048]{1,0:T(8,128)(2,1)S(1)}, bf16[128,2048]{1,0:T(8,128)(2,1)}, u32[]{:S(2)}) copy-start(bf16[128,2048]{1,0:T(8,128)(2,1)} %param.31) | copy-start | bytes 1572868
Sparse Core Ops, SparseCore 0:
  9.2 42.3 all-gather.1
  152.8 36.4 reduce-scatter.1
where the time goes:
time: 199 us; the launch traced here: 196 us
  waiting for transfers between devices  80.6 us (41%)
  local copies, waits for them, and re-layouts  30.1 us (15%)
  other arithmetic  24.7 us (12%)
  matrix products  21.6 us (11%)
  starting transfers between devices  21.5 us (11%)
  between operations  17.2 us (9%)
    reduce_scatter x1, waiting for transfers between devices, body(): lax.psum_scatter((att_part + lax.dot_general(out_ret, ret_out, contract_d...  36.6 us
    all_gather x1, waiting for transfers between devices, body(): lax.all_gather(tokens, 'tp', axis=1, tiled=True).astype(jnp.float32)  24.7 us
    all_to_all x2, waiting for transfers between devices, copy_for_each(): return lax.all_to_all(copies, axis, split_axis=0, concat_axis=0, tiled=True)  18.6 us
    all_to_all x2, starting transfers between devices, copy_for_each(): return lax.all_to_all(copies, axis, split_axis=0, concat_axis=0, tiled=True)  17.1 us
    unnamed x40, local copies, waits for them, and re-layouts  10.5 us
    dynamic_slice x16, local copies, waits for them, and re-layouts, body(): fwd_total, fwd_local = lax.scan(advance, zero_state, (factors, fwd_terms))  9.36 us
    add x16, other arithmetic, advance(): return (factor_now[:, None, None] * state_now + term_now, state_now)  9.04 us
    dot_general x1, matrix products, body(): lax.dot_general(out_ret, ret_out, contract_dims, preferred_element_type=j...  6.77 us
  transfers between devices with their start and end apart: 6, of which 4 were waited for; matrix products, arithmetic and copies ran while one was open for 27% of the time, Pallas kernels for 0%

commit v1 on v0

v1 whole, which is shorter than its diff:
```python
import functools

import jax
import jax.numpy as jnp
import numpy as np
from jax import lax
from jax.experimental import pallas as pl
from jax.experimental.pallas import tpu as pltpu
from jax.sharding import PartitionSpec as P

HD = 64
RV = 128
BLK = 128
NORM_EPS = 1e-06
ROPE_BASE = 10000.0
MESH = pl.DeviceIdType.MESH
F32 = jnp.float32
BF16 = jnp.bfloat16
NT = (((1,), (1,)), ((), ()))
TN = (((0,), (0,)), ((), ()))

L1, R1, OPP, SIB = 0, 1, 2, 3


def kernel(n_sp, nx, tok_h, gain_h, wq_h, wk_h, wv_h, wrq_h, wrk_h, wrv_h, wrg_h, sink_ref, dec_h, init_h, inv_h, oa_h, or_h,
           out_h,
           X, W1, W2, gain, dec, init, inv, Q, KV, V, G, QR, QB, QX, RL, TT, SL, A, R, WO, OA, OUT,
           XS, ZG, ZS, DX, DZ, crow, bl8, pre8,
           lsem, xs_s, xs_r, as_s, as_r, rs_s, rs_r, w1_s, w1_r, w2_s, w2_r, sx_s, sx_r, dx_s, dx_r, sz_s, sz_r, dz_s, dz_r,
           h_s, h_r):
    rows, cw = tok_h.shape
    nb = rows // BLK
    arows = 2 * BLK
    na = rows // arows
    width = 8 * cw
    ocw = OUT.shape[1]
    nz = n_sp // nx
    quarter = BLK // nx
    s, t = lax.axis_index("sp"), lax.axis_index("tp")
    z, x = s // nx, s % nx
    y, c = t // 2, t % 2
    right = 2 * ((y + 1) % 4) + c
    left = 2 * ((y + 3) % 4) + c
    opp = 2 * ((y + 2) % 4) + c
    sib = 2 * y + (1 - c)
    up, down = (s + 1) % n_sp, (s + n_sp - 1) % n_sp

    loads = [
        (dec_h, dec), (tok_h, X.at[t]), (gain_h, gain), (inv_h, inv), (init_h, init),
        (wq_h, W1.at[:, 0:128]), (wrv_h, W1.at[:, 128:256]), (wrg_h, W1.at[:, 256:384]),
        (wk_h, W2.at[0:64]), (wv_h, W2.at[64:128]), (wrq_h, W2.at[128:192]), (wrk_h, W2.at[192:256]),
    ]
    mine = pl.ds(pl.multiple_of(x * quarter, quarter), quarter)
    my_cols = pl.ds(pl.multiple_of(t * ocw, 128), ocw)
    loads += [(oa_h.at[mine, my_cols], WO.at[0, t, mine, :]), (or_h.at[mine, my_cols], WO.at[1, t, mine, :])]
    copies = [pltpu.make_async_copy(a, b, lsem.at[i]) for i, (a, b) in enumerate(loads)]
    for cp in copies:
        cp.start()

    barrier = pltpu.get_barrier_semaphore()
    partners = [(s, (t + d) % 8) for d in range(1, 8)]
    partners += [(z * nx + (x + d) % nx, t) for d in range(1, nx)]
    partners += [(((z + d) % nz) * nx + x, t) for d in range(1, nz)]
    partners += [(up, t), (down, t)]
    for p in partners:
        pl.semaphore_signal(barrier, inc=1, device_id=p, device_id_type=MESH)

    copies[0].wait()
    for b in range(nb):
        crow[b : b + 1, :] = dec[:, b * BLK : (b + 1) * BLK]
    cum = crow[...]
    lane = lax.broadcasted_iota(jnp.int32, (nb, BLK), 1)
    for sh in (1, 2, 4, 8, 16, 32, 64):
        cum = cum + jnp.where(lane >= sh, pltpu.roll(cum, sh, 1), 0.0)
    crow[...] = cum
    bl8[...] = jnp.broadcast_to(cum[:, BLK - 1 : BLK], (nb, BLK))
    run = jnp.zeros((1, BLK), F32)
    for b in range(nb):
        pre8[b : b + 1, :] = run
        run = run + bl8[b : b + 1, :]
    tot = run
    DX[x] = jnp.broadcast_to(tot, (8, BLK))
    for i in range(1, 5):
        copies[i].wait()

    pl.semaphore_wait(barrier, len(partners))

    def put(src, dst, send, recv, dev):
        return pltpu.make_async_remote_copy(src_ref=src, dst_ref=dst, send_sem=send, recv_sem=recv, device_id=dev, device_id_type=MESH)

    def gather(buf, n_rows, ss, rs):
        def part(b, k):
            return buf.at[b, pl.ds(pl.multiple_of(k * n_rows, n_rows), n_rows), :]

        def hop(b, k, send, recv, tp):
            ref = part(b, k)
            return put(ref, ref, ss.at[send, k], rs.at[recv, k], (s, tp))

        def own(k):
            hop(t, k, 0, L1, right).start()
            hop(t, k, 1, R1, left).start()
            hop(t, k, 2, SIB, sib).start()

        def pass_on(k):
            hop(left, k, 3, L1, right).wait_recv()
            even = k % 2 == 0

            @pl.when(even)
            def _():
                hop(left, k, 6, OPP, right).start()

            hop(left, k, 3, SIB + 1, sib).start()
            hop(right, k, 4, R1, left).wait_recv()

            @pl.when(k % 2 == 1)
            def _():
                hop(right, k, 6, OPP, left).start()

            hop(right, k, 4, SIB + 2, sib).start()

        def pass_last(k):
            hop(opp, k, 5, OPP, right).wait_recv()
            hop(opp, k, 5, SIB + 3, sib).start()

        def arrived(k):
            hop(sib, k, 2, SIB, sib).wait_recv()
            hop(2 * ((y + 3) % 4) + 1 - c, k, 3, SIB + 1, sib).wait_recv()
            hop(2 * ((y + 1) % 4) + 1 - c, k, 4, SIB + 2, sib).wait_recv()
            hop(2 * ((y + 2) % 4) + 1 - c, k, 5, SIB + 3, sib).wait_recv()

        def sent(k):
            for i in range(7):
                hop(t, k, i, L1, right).wait_send()

        return own, pass_on, pass_last, arrived, sent

    own, pass_on, pass_last, arrived, sent = gather(X, BLK, xs_s, xs_r)
    a_own, a_pass, a_last, a_arrived, a_sent = gather(A, arows, as_s, as_r)
    r_own, r_pass, r_last, r_arrived, r_sent = gather(R, arows, rs_s, rs_r)

    own(0)
    own(1)
    for d in range(1, nx):
        put(DX.at[x], DX.at[x], dx_s.at[d], dx_r.at[d], (z * nx + (x + d) % nx, t)).start()

    lane_b = lax.broadcasted_iota(jnp.int32, (BLK, BLK), 1)
    row_b = lax.broadcasted_iota(jnp.int32, (BLK, BLK), 0)
    low = lane_b < 64

    def blk(j):
        return pl.ds(pl.multiple_of(j * BLK, BLK), BLK)

    def column(j):
        row = jnp.broadcast_to(crow[pl.ds(j, 1), :], (BLK, BLK))
        return jnp.sum(jnp.where(lane_b == row_b, row, 0.0), axis=1, keepdims=True)

    def project(j):
        pos = (s * rows + j * BLK + row_b).astype(F32)
        angle = pos * inv[...]
        scale = jnp.where(low, 1.0, 64**-0.5).astype(F32)
        cosine = jnp.cos(angle) * scale
        sine = jnp.sin(angle) * jnp.where(lane_b % 64 < 32, -scale, scale)
        cc = column(j)
        bl = bl8[pl.ds(j, 1), :]
        pre = pre8[pl.ds(j, 1), :]
        arrived(j)
        squares = jnp.zeros((BLK, cw), F32)
        parts = []
        for b in range(8):
            xf = X[b, blk(j), :].astype(F32)
            squares = squares + xf * xf
            parts.append((xf * gain[:, b * cw : (b + 1) * cw]).astype(BF16))
        normed = jnp.concatenate(parts, axis=1)
        inv_rms = lax.rsqrt(jnp.sum(squares, axis=1, keepdims=True) / width + NORM_EPS)
        p1 = (jnp.dot(normed, W1[...], preferred_element_type=F32) * inv_rms).astype(BF16)
        p2 = (lax.dot_general(normed, W2[...], NT, preferred_element_type=F32) * inv_rms).astype(BF16)
        Q[blk(j), :] = p1[:, 0:128]
        v = p1[:, 128:256]
        V[blk(j), :] = v
        G[blk(j), :] = p1[:, 256:384]
        KV[blk(j + 1), :] = p2[:, 0:128]
        rqk = p2[:, 128:256].astype(F32)
        swapped = jnp.where(lane_b % 64 < 32, pltpu.roll(rqk, 96, 1), pltpu.roll(rqk, 32, 1))
        rot = rqk * cosine + swapped * sine
        QR[blk(j), :] = rot.astype(BF16)
        other = pltpu.roll(rot, 64, 1)
        qq = jnp.where(low, rot, other)
        kk = jnp.where(low, other, rot)
        to_end = jnp.exp(bl - cc)
        to_here = jnp.exp(jnp.broadcast_to(cc, (BLK, BLK)))
        QB[blk(j), :] = (qq * jnp.where(low, to_here, to_end)).astype(BF16)
        full = cc + pre
        QX[blk(j), :] = (qq * jnp.exp(jnp.where(low, full, tot - full))).astype(BF16)
        kw = (kk * jnp.where(low, to_end, to_here)).astype(BF16)
        TT[j] = lax.dot_general(kw, v, TN, preferred_element_type=F32)

    for i in range(5, 12):
        copies[i].wait()

    def step(k, carry):
        @pl.when(k < nb - 2)
        def _():
            own(k + 2)

        @pl.when(k < nb)
        def _():
            pass_on(k)

        @pl.when((k >= 1) & (k < nb + 1))
        def _():
            pass_last(k - 1)

        @pl.when(k >= 2)
        def _():
            project(k - 2)

        return carry

    lax.fori_loop(0, nb + 2, step, 0)

    halo_up = put(KV.at[pl.ds(rows, BLK), :], KV.at[pl.ds(0, BLK), :], h_s.at[0], h_r.at[0], (up, t))
    halo_down = put(KV.at[pl.ds(BLK, BLK), :], KV.at[pl.ds(rows + BLK, BLK), :], h_s.at[1], h_r.at[1], (down, t))
    halo_up.start()
    halo_down.start()

    f = jnp.zeros((64, RV), F32)
    g = jnp.zeros((64, RV), F32)
    for b in range(nb):
        SL[b, 0:64, :] = f.astype(BF16)
        f = jnp.exp(bl8[b : b + 1, :]) * f + TT[b, 0:64, :]
        e = nb - 1 - b
        SL[e, 64:128, :] = g.astype(BF16)
        g = jnp.exp(bl8[e : e + 1, :]) * g + TT[e, 64:128, :]
    XS[x, 0:64, :] = f.astype(BF16)
    XS[x, 64:128, :] = g.astype(BF16)
    for d in range(1, nx):
        put(XS.at[x], XS.at[x], sx_s.at[d], sx_r.at[d], (z * nx + (x + d) % nx, t)).start()
    for d in range(1, nx):
        put(DX.at[(x + nx - d) % nx], DX.at[(x + nx - d) % nx], dx_s.at[d], dx_r.at[d], (s, sib)).wait_recv()
    total = DX[0]
    for i in range(1, nx):
        total = total + DX[i]
    DZ[z] = total
    for d in range(1, nz):
        put(DZ.at[z], DZ.at[z], dz_s.at[d], dz_r.at[d], (((z + d) % nz) * nx + x, t)).start()

    copies[12].wait()
    copies[13].wait()
    for d in range(1, 8):
        to = (t + d) % 8
        cols = pl.ds(pl.multiple_of(to * ocw, 128), ocw)
        put(oa_h.at[mine, cols], WO.at[0, t, mine, :], w1_s.at[0, d], w1_r.at[0, d], (s, to)).start()
        put(or_h.at[mine, cols], WO.at[1, t, mine, :], w1_s.at[1, d], w1_r.at[1, d], (s, to)).start()

    row_q = lax.broadcasted_iota(jnp.int32, (2 * BLK, BLK), 0) % BLK
    lane_q = lax.broadcasted_iota(jnp.int32, (2 * BLK, BLK), 1)
    sink = jnp.where(lax.broadcasted_iota(jnp.int32, (2 * BLK, 1), 0) < BLK, sink_ref[0], sink_ref[1])

    def attend(i, carry):
        j = (i + 2) % nb

        @pl.when(i == nb - 2)
        def _():
            halo_up.wait_recv()

        @pl.when(i == nb - 3)
        def _():
            halo_down.wait_recv()

        q = Q[blk(j), :]
        q2 = jnp.concatenate([q[:, 0:64], q[:, 64:128]], axis=0)
        kv = KV[pl.ds(pl.multiple_of(j * BLK, BLK), 3 * BLK), :]
        sc = lax.dot_general(q2, kv[:, 0:64], NT, preferred_element_type=F32) * HD**-0.5
        first = jnp.where(s * nb + j == 0, BLK, 0)
        last = jnp.where(s * nb + j == n_sp * nb - 1, BLK, 0)
        s0 = jnp.where(lane_q - first >= row_q, sc[:, 0:128], -jnp.inf)
        s1 = sc[:, 128:256]
        s2 = jnp.where(lane_q + last <= row_q, sc[:, 256:384], -jnp.inf)
        top = jnp.maximum(jnp.max(jnp.maximum(jnp.maximum(s0, s1), s2), axis=1, keepdims=True), sink)
        e0, e1, e2 = jnp.exp(s0 - top), jnp.exp(s1 - top), jnp.exp(s2 - top)
        den = jnp.sum(e0 + e1 + e2, axis=1, keepdims=True) + jnp.exp(sink - top)
        ee = jnp.concatenate([e0.astype(BF16), e1.astype(BF16), e2.astype(BF16)], axis=1)
        o = jnp.dot(ee, kv[:, 64:128], preferred_element_type=F32) / den
        A[t, blk(j), :] = jnp.concatenate([o[0:BLK], o[BLK : 2 * BLK]], axis=1).astype(BF16)

        @pl.when(i % 2 == 1)
        def _():
            a_own(j // 2)

        return carry

    lax.fori_loop(0, nb, attend, 0)

    for d in range(1, nx):
        o = (x + nx - d) % nx
        put(XS.at[o], XS.at[o], sx_s.at[d], sx_r.at[d], (s, sib)).wait_recv()
    ex = [jnp.exp(DX[i][0:1, :]) for i in range(nx)]
    fx = jnp.zeros((64, RV), F32)
    gx = jnp.zeros((64, RV), F32)
    fall = jnp.zeros((64, RV), F32)
    gall = jnp.zeros((64, RV), F32)
    dfx = jnp.zeros((1, RV), F32)
    dgx = jnp.zeros((1, RV), F32)
    for i in range(nx):
        term = XS[i, 0:64, :].astype(F32)
        fx = jnp.where(i < x, ex[i] * fx + term, fx)
        dfx = jnp.where(i < x, dfx + DX[i][0:1, :], dfx)
        fall = ex[i] * fall + term
        o = nx - 1 - i
        term = XS[o, 64:128, :].astype(F32)
        gx = jnp.where(o > x, ex[o] * gx + term, gx)
        dgx = jnp.where(o > x, dgx + DX[o][0:1, :], dgx)
        gall = ex[o] * gall + term
    ZG[0] = fall.astype(BF16)
    ZG[1] = gall.astype(BF16)
    ZS[z] = jnp.zeros((64, RV), BF16)
    for d in range(1, nz):
        put(ZG.at[(z + d) // nz], ZS.at[z], sz_s.at[d], sz_r.at[d], (((z + d) % nz) * nx + x, t)).start()

    a_order = [(i + 1) % na for i in range(na)]
    for k in a_order:
        a_pass(k)

    def inside(j, carry):
        cc = column(j)
        cr = crow[pl.ds(j, 1), :]
        qk = QR[blk(j), :]
        sc = lax.dot_general(qk[:, 0:64], qk[:, 64:128], NT, preferred_element_type=F32)
        w = (sc * jnp.exp(-jnp.abs(cc - cr))).astype(BF16)
        RL[blk(j), :] = jnp.dot(w, V[blk(j), :], preferred_element_type=F32) + jnp.dot(
            QB[blk(j), :], SL[j], preferred_element_type=F32
        )
        return carry

    lax.fori_loop(0, nb, inside, 0)

    for d in range(1, 8):
        fr = (t + 8 - d) % 8
        for i in range(2):
            ref = WO.at[i, fr, mine, :]
            put(ref, ref, w1_s.at[i, d], w1_r.at[i, d], (s, sib)).wait_recv()
    for d in range(1, nx):
        ref = WO.at[:, :, mine, :]
        put(ref, ref, w2_s.at[d], w2_r.at[d], (z * nx + (x + d) % nx, t)).start()

    for k in a_order:
        a_last(k)

    for d in range(1, nz):
        o = (z + nz - d) % nz
        put(DZ.at[o], DZ.at[o], dz_s.at[d], dz_r.at[d], (s, sib)).wait_recv()
        put(ZS.at[o], ZS.at[o], sz_s.at[d], sz_r.at[d], (s, sib)).wait_recv()
    fz = init[0:64, :]
    gz = init[64:128, :]
    for i in range(nz):
        term = ZS[i].astype(F32)
        fz = jnp.where(i < z, jnp.exp(DZ[i][0:1, :]) * fz + term, fz)
        o = nz - 1 - i
        term = ZS[o].astype(F32)
        gz = jnp.where(o > z, jnp.exp(DZ[o][0:1, :]) * gz + term, gz)
    ST = jnp.concatenate([fx + jnp.exp(dfx) * fz, gx + jnp.exp(dgx) * gz], axis=0).astype(BF16)

    def finish(j, carry):
        ret = RL[blk(j), :] + jnp.dot(QX[blk(j), :], carry, preferred_element_type=F32)
        cen = ret - jnp.mean(ret, axis=1, keepdims=True)
        nrm = cen * lax.rsqrt(jnp.mean(cen * cen, axis=1, keepdims=True) + NORM_EPS)
        gate = G[blk(j), :].astype(F32)
        R[t, blk(j), :] = (gate / (1.0 + jnp.exp(-gate)) * nrm).astype(BF16)

        @pl.when(j % 2 == 1)
        def _():
            r_own(j // 2)

        return carry

    lax.fori_loop(0, nb, finish, ST)

    for k in range(na):
        r_pass(k)

    for k in range(na):
        a_arrived(k)
    for d in range(1, nx):
        ref = WO.at[:, :, pl.ds(pl.multiple_of(((x + nx - d) % nx) * quarter, quarter), quarter), :]
        put(ref, ref, w2_s.at[d], w2_r.at[d], (s, sib)).wait_recv()

    def big(k):
        return pl.ds(pl.multiple_of(k * arows, arows), arows)

    def out_att(k, carry):
        lhs = jnp.concatenate([A[b, big(k), :] for b in range(8)], axis=1)
        OA[big(k), :] = jnp.dot(lhs, WO[0].reshape(8 * BLK, ocw), preferred_element_type=F32)
        return carry

    lax.fori_loop(0, na, out_att, 0)

    for k in range(na):
        r_last(k)

    def out_ret(k, carry):
        r_arrived(k)
        lhs = jnp.concatenate([R[b, big(k), :] for b in range(8)], axis=1)
        acc = OA[big(k), :] + jnp.dot(lhs, WO[1].reshape(8 * BLK, ocw), preferred_element_type=F32)
        OUT[big(k), :] = acc.astype(BF16)
        pltpu.make_async_copy(OUT.at[big(k), :], out_h.at[big(k), :], lsem.at[14 + k]).start()
        return carry

    lax.fori_loop(0, na, out_ret, 0)

    def drain(k, carry):
        sent(k)
        return carry

    lax.fori_loop(0, nb, drain, 0)
    for k in range(na):
        a_sent(k)
        r_sent(k)
        pltpu.make_async_copy(OUT.at[big(k), :], out_h.at[big(k), :], lsem.at[14 + k]).wait()
    for d in range(1, 8):
        for i in range(2):
            put(oa_h.at[mine, my_cols], WO.at[i, t, mine, :], w1_s.at[i, d], w1_r.at[i, d], (s, sib)).wait_send()
    for d in range(1, nx):
        ref = WO.at[:, :, mine, :]
        put(ref, ref, w2_s.at[d], w2_r.at[d], (s, sib)).wait_send()
        put(XS.at[x], XS.at[x], sx_s.at[d], sx_r.at[d], (s, sib)).wait_send()
        put(DX.at[x], DX.at[x], dx_s.at[d], dx_r.at[d], (s, sib)).wait_send()
    for d in range(1, nz):
        put(ZG.at[0], ZS.at[z], sz_s.at[d], sz_r.at[d], (s, sib)).wait_send()
        put(DZ.at[z], DZ.at[z], dz_s.at[d], dz_r.at[d], (s, sib)).wait_send()
    halo_up.wait_send()
    halo_down.wait_send()


def body(tokens, norm_gain, att_query, att_key, att_value, ret_query, ret_key, ret_value, ret_gate, att_sink, decay_log, init_state,
         out_att, out_ret, *, n_sp):
    rows, cw = tokens.shape
    width = 8 * cw
    ocw = out_att.shape[1] // 8
    nb, na = rows // BLK, rows // (2 * BLK)
    nx = 4 if n_sp >= 16 else 2
    nz = n_sp // nx
    inverse = (np.float64(ROPE_BASE) ** (-2.0 * (np.arange(128) % 32) / 64)).astype(np.float32)[None, :]
    dma = pltpu.SemaphoreType.DMA
    hbm = pl.BlockSpec(memory_space=pltpu.HBM)
    specs = [hbm] * 15
    specs[9] = pl.BlockSpec(memory_space=pltpu.SMEM)
    vm = pltpu.VMEM
    scratch = [
        vm((8, rows, cw), BF16), vm((width, 384), BF16), vm((256, width), BF16), vm((1, width), F32), vm((1, rows), F32),
        vm((128, 128), F32), vm((1, 128), F32),
        vm((rows, 128), BF16), vm((rows + 2 * BLK, 128), BF16), vm((rows, 128), BF16), vm((rows, 128), BF16),
        vm((rows, 128), BF16), vm((rows, 128), BF16), vm((rows, 128), BF16), vm((rows, 128), F32),
        vm((nb, 128, 128), F32), vm((nb, 128, 128), BF16),
        vm((8, rows, 128), BF16), vm((8, rows, 128), BF16), vm((2, 8, 128, ocw), BF16), vm((rows, ocw), F32), vm((rows, ocw), BF16),
        vm((nx, 128, 128), BF16), vm((2, 64, 128), BF16), vm((nz, 64, 128), BF16), vm((nx, 8, 128), F32), vm((nz, 8, 128), F32),
        vm((nb, 128), F32), vm((nb, 128), F32), vm((nb, 128), F32),
        dma((14 + na,)), dma((7, nb)), dma((7, nb)), dma((7, na)), dma((7, na)), dma((7, na)), dma((7, na)),
        dma((2, 8)), dma((2, 8)), dma((nx,)), dma((nx,)), dma((nx,)), dma((nx,)), dma((nx,)), dma((nx,)),
        dma((max(nz, 2),)), dma((max(nz, 2),)), dma((max(nz, 2),)), dma((max(nz, 2),)), dma((2,)), dma((2,)),
    ]
    call = pl.pallas_call(
        functools.partial(kernel, n_sp, nx),
        out_shape=jax.ShapeDtypeStruct((rows, ocw), BF16),
        in_specs=specs,
        out_specs=hbm,
        scratch_shapes=scratch,
        compiler_params=pltpu.CompilerParams(collective_id=0, has_side_effects=True, vmem_limit_bytes=48 * 1024 * 1024),
        name="layer",
    )
    return call(
        tokens, norm_gain.reshape(1, width), att_query, att_key.T, att_value.T, ret_query.T, ret_key.T, ret_value, ret_gate,
        att_sink, decay_log, init_state.reshape(128, 128), inverse, out_att, out_ret,
    )


def solution(mesh):
    in_specs = (
        P("sp", "tp"), P(), P(None, "tp"), P(None, "tp"), P(None, "tp"), P(None, "tp"), P(None, "tp"), P(None, "tp"), P(None, "tp"),
        P("tp"), P("tp", "sp"), P(None, "tp", None, None), P("tp", None), P("tp", None),
    )
    return jax.shard_map(
        functools.partial(body, n_sp=mesh.shape["sp"]), mesh=mesh, in_specs=in_specs, out_specs=P("sp", "tp"), check_vma=False
    )
```

time: 199 us -> 89.1 us (0.45); the launches traced: 196 us -> 88.5 us
  waiting for transfers between devices: 80.6 us -> 0 us
  Pallas kernels: 0 us -> 75.4 us
  other arithmetic: 24.7 us -> 0 us
  matrix products: 21.6 us -> 0 us
  starting transfers between devices: 21.5 us -> 0 us
  between operations: 17.2 us -> 0.03 us
  local copies, waits for them, and re-layouts: 30.1 us -> 13.1 us
    pallas_call x0 -> x1, Pallas kernels: none -> 75.4 us  [body(): call(tokens, norm_gain.reshape(1, width), att_query, att_key.T, att_value...]
    reduce_scatter x1 -> x0, waiting for transfers between devices: 36.6 us -> none  [body(): lax.psum_scatter((att_part + lax.dot_general(out_ret, ret_out, contract_d...]
    all_gather x1 -> x0, waiting for transfers between devices: 24.7 us -> none  [body(): lax.all_gather(tokens, 'tp', axis=1, tiled=True).astype(jnp.float32)]
    dot_general x12 -> x0, matrix products: 21.6 us -> none  [the longest x1 6.77 us: body(): lax.dot_general(out_ret, ret_out, contract_dims, preferred_element_type=j...]
    all_to_all x2 -> x0, waiting for transfers between devices: 18.6 us -> none  [copy_for_each(): return lax.all_to_all(copies, axis, split_axis=0, concat_axis=0, tiled=True)]
    all_to_all x2 -> x0, starting transfers between devices: 17.1 us -> none  [copy_for_each(): return lax.all_to_all(copies, axis, split_axis=0, concat_axis=0, tiled=True)]
    add x30 -> x0, other arithmetic: 9.95 us -> none  [the longest x16 9.04 us: advance(): return (factor_now[:, None, None] * state_now + term_now, state_now)]
    dynamic_slice x16 -> x0, local copies, waits for them, and re-layouts: 9.36 us -> none  [body(): fwd_total, fwd_local = lax.scan(advance, zero_state, (factors, fwd_terms))]
  transfers between devices with their start and end apart: 6 -> 0, of which waited for: 4 -> 0; matrix products, arithmetic and copies ran while one was open for 27% -> 0% of each run, Pallas kernels for 0% -> 0%
where the time goes in v1:
time: 89.1 us; the launch traced here: 88.5 us
  Pallas kernels  75.4 us (85%)
  local copies, waits for them, and re-layouts  13.1 us (15%)
    pallas_call x1, Pallas kernels, body(): call(tokens, norm_gain.reshape(1, width), att_query, att_key.T, att_value...  75.4 us
    unnamed x31, local copies, waits for them, and re-layouts  13.1 us

profile of v1, /device:TPU:1, one launch (start us, length us, event | category | flops | bytes accessed | tf_op | source)
XLA Modules:
  0.0 88.5 jit_solution(10582167790801399278)
XLA Ops:
  0.0 0.0 copy-start.11
  0.0 0.0 copy-start.13
  0.0 0.0 copy-start.14
  0.0 0.7 copy-done.11
  0.7 0.0 copy-done.13
  0.7 0.0 copy-done.14
  0.7 0.0 copy-start
  0.7 1.0 %copy-done = bf16[1024,256]{1,0:T(8,128)(2,1)S(1)} copy-done((bf16[1024,256]{1,0:T(8,128)(2,1)S(1)}, bf16[1024,256]{1,0:T(8,128)(2,1)}, u32[]{:S(2)}) %copy-start) | copy-done | bytes 524312
  1.7 0.0 copy-start.1
  1.7 1.0 %copy-done.1 = bf16[2048,128]{1,0:T(8,128)(2,1)S(1)} copy-done((bf16[2048,128]{1,0:T(8,128)(2,1)S(1)}, bf16[2048,128]{1,0:T(8,128)(2,1)}, u32[]{:S(2)}) %copy-start.1) | copy-done | bytes 524312
  2.8 0.0 copy-start.2
  2.8 1.0 %copy-done.2 = bf16[2048,128]{1,0:T(8,128)(2,1)S(1)} copy-done((bf16[2048,128]{1,0:T(8,128)(2,1)S(1)}, bf16[2048,128]{1,0:T(8,128)(2,1)}, u32[]{:S(2)}) %copy-start.2) | copy-done | bytes 524312
  3.8 0.0 copy-start.3
  3.8 1.0 %copy-done.3 = bf16[2048,128]{1,0:T(8,128)(2,1)S(1)} copy-done((bf16[2048,128]{1,0:T(8,128)(2,1)S(1)}, bf16[2048,128]{1,0:T(8,128)(2,1)}, u32[]{:S(2)}) %copy-start.3) | copy-done | bytes 524312
  4.9 0.0 copy-start.4
  4.9 1.0 %copy-done.4 = bf16[128,2048]{1,0:T(8,128)(2,1)S(1)} copy-done((bf16[128,2048]{1,0:T(8,128)(2,1)S(1)}, bf16[128,2048]{1,0:T(8,128)(2,1)}, u32[]{:S(2)}) %copy-start.4) | copy-done | bytes 524312
  5.9 0.0 copy-start.5
  5.9 1.0 %copy-done.5 = bf16[128,2048]{1,0:T(8,128)(2,1)S(1)} copy-done((bf16[128,2048]{1,0:T(8,128)(2,1)S(1)}, bf16[128,2048]{1,0:T(8,128)(2,1)}, u32[]{:S(2)}) %copy-start.5) | copy-done | bytes 524312
  7.0 0.0 copy-start.6
  7.0 0.9 %copy-done.6 = bf16[2048,64]{0,1:T(8,128)(2,1)S(1)} copy-done((bf16[2048,64]{0,1:T(8,128)(2,1)S(1)}, bf16[2048,64]{0,1:T(8,128)(2,1)}, u32[]{:S(2)}) %copy-start.6) | copy-done | bytes 262168
  7.9 0.0 copy-start.7
  7.9 0.9 %copy-done.7 = bf16[2048,64]{0,1:T(8,128)(2,1)S(1)} copy-done((bf16[2048,64]{0,1:T(8,128)(2,1)S(1)}, bf16[2048,64]{0,1:T(8,128)(2,1)}, u32[]{:S(2)}) %copy-start.7) | copy-done | bytes 262168
  8.9 0.0 copy-start.8
  8.9 0.9 %copy-done.8 = bf16[2048,64]{0,1:T(8,128)(2,1)S(1)} copy-done((bf16[2048,64]{0,1:T(8,128)(2,1)S(1)}, bf16[2048,64]{0,1:T(8,128)(2,1)}, u32[]{:S(2)}) %copy-start.8) | copy-done | bytes 262168
  9.8 0.0 copy-start.9
  9.8 0.9 %copy-done.9 = bf16[2048,64]{0,1:T(8,128)(2,1)S(1)} copy-done((bf16[2048,64]{0,1:T(8,128)(2,1)S(1)}, bf16[2048,64]{0,1:T(8,128)(2,1)}, u32[]{:S(2)}) %copy-start.9) | copy-done | bytes 262168
  10.8 0.0 copy-start.10
  10.8 0.8 copy-done.10
  11.6 0.0 copy-start.12
  11.6 0.7 copy-done.12
  12.3 75.4 %layer.1 = bf16[1024,256]{1,0:T(8,128)(2,1)S(1)} custom-call(bf16[1024,256]{1,0:T(8,128)(2,1)S(1)} %copy-done, f32[1,2048]{1,0:T(1,128)S(1)} %bitcast.11, bf16[2048,128]{1,0:T(8,128)(2,1)S(1)} %copy-done.1, bf16[64,2048]{1,0:T(8,128)(2,1)S(1)} %bitcast.6, bf16[64,2048]{1,0:T(8,128)(2,1)S(1)} %bitcast.7, bf16[64,2048]{1,0:T(8,128)(2,1)S(1)} %bitcast.8, ...), custom_call_target="tpu_custom_call" | custom-call | tf_op jit(solution)/shard_map/layer/pallas_call | solution.py:470
  87.7 0.8 copy.17
Async XLA Ops:
  0.0 0.7 copy-start.11
  0.0 0.7 copy-start.13
  0.0 0.7 copy-start.14
  0.7 1.0 %copy-start = (bf16[1024,256]{1,0:T(8,128)(2,1)S(1)}, bf16[1024,256]{1,0:T(8,128)(2,1)}, u32[]{:S(2)}) copy-start(bf16[1024,256]{1,0:T(8,128)(2,1)} %tok_h.1) | copy-start | bytes 1572868
  1.7 1.0 %copy-start.1 = (bf16[2048,128]{1,0:T(8,128)(2,1)S(1)}, bf16[2048,128]{1,0:T(8,128)(2,1)}, u32[]{:S(2)}) copy-start(bf16[2048,128]{1,0:T(8,128)(2,1)} %wq_h.1) | copy-start | bytes 1572868
  2.8 1.0 %copy-start.2 = (bf16[2048,128]{1,0:T(8,128)(2,1)S(1)}, bf16[2048,128]{1,0:T(8,128)(2,1)}, u32[]{:S(2)}) copy-start(bf16[2048,128]{1,0:T(8,128)(2,1)} %wrv_h.1) | copy-start | bytes 1572868
  3.8 1.0 %copy-start.3 = (bf16[2048,128]{1,0:T(8,128)(2,1)S(1)}, bf16[2048,128]{1,0:T(8,128)(2,1)}, u32[]{:S(2)}) copy-start(bf16[2048,128]{1,0:T(8,128)(2,1)} %wrg_h.1) | copy-start | bytes 1572868
  4.9 1.0 %copy-start.4 = (bf16[128,2048]{1,0:T(8,128)(2,1)S(1)}, bf16[128,2048]{1,0:T(8,128)(2,1)}, u32[]{:S(2)}) copy-start(bf16[128,2048]{1,0:T(8,128)(2,1)} %oa_h.1) | copy-start | bytes 1572868
  5.9 1.0 %copy-start.5 = (bf16[128,2048]{1,0:T(8,128)(2,1)S(1)}, bf16[128,2048]{1,0:T(8,128)(2,1)}, u32[]{:S(2)}) copy-start(bf16[128,2048]{1,0:T(8,128)(2,1)} %or_h.1) | copy-start | bytes 1572868
  7.0 0.9 %copy-start.6 = (bf16[2048,64]{0,1:T(8,128)(2,1)S(1)}, bf16[2048,64]{0,1:T(8,128)(2,1)}, u32[]{:S(2)}) copy-start(bf16[2048,64]{0,1:T(8,128)(2,1)} %param.18) | copy-start | bytes 786436
  7.9 0.9 %copy-start.7 = (bf16[2048,64]{0,1:T(8,128)(2,1)S(1)}, bf16[2048,64]{0,1:T(8,128)(2,1)}, u32[]{:S(2)}) copy-start(bf16[2048,64]{0,1:T(8,128)(2,1)} %param.19) | copy-start | bytes 786436
  8.9 0.9 %copy-start.8 = (bf16[2048,64]{0,1:T(8,128)(2,1)S(1)}, bf16[2048,64]{0,1:T(8,128)(2,1)}, u32[]{:S(2)}) copy-start(bf16[2048,64]{0,1:T(8,128)(2,1)} %param.20) | copy-start | bytes 786436
  9.8 0.9 %copy-start.9 = (bf16[2048,64]{0,1:T(8,128)(2,1)S(1)}, bf16[2048,64]{0,1:T(8,128)(2,1)}, u32[]{:S(2)}) copy-start(bf16[2048,64]{0,1:T(8,128)(2,1)} %param.21) | copy-start | bytes 786436
  10.8 0.8 copy-start.10
  11.6 0.7 copy-start.12

commit v2 on v1

--- a/solution.py
+++ b/solution.py
@@ -464,7 +464,7 @@
         in_specs=specs,
         out_specs=hbm,
         scratch_shapes=scratch,
-        compiler_params=pltpu.CompilerParams(collective_id=0, has_side_effects=True, vmem_limit_bytes=48 * 1024 * 1024),
+        compiler_params=pltpu.CompilerParams(collective_id=0, has_side_effects=True, vmem_limit_bytes=67_043_328),
         name="layer",
     )
     return call(

time: 89.1 us -> 76.8 us (0.86)
  local copies, waits for them, and re-layouts: 13.1 us -> 1.87 us
    unnamed x31 -> x1, local copies, waits for them, and re-layouts: 13.1 us -> 1.87 us
where the time goes in v2:
time: 76.8 us; the launch traced here: 76.6 us
  Pallas kernels  74.8 us (97%)
  local copies, waits for them, and re-layouts  1.87 us (2%)
    pallas_call x1, Pallas kernels, body(): call(tokens, norm_gain.reshape(1, width), att_query, att_key.T, att_value...  74.8 us
    unnamed x1, local copies, waits for them, and re-layouts  1.87 us

profile of v2, /device:TPU:1, one launch (start us, length us, event | category | flops | bytes accessed | tf_op | source)
XLA Modules:
  0.0 76.6 jit_solution(283504463327445909)
XLA Ops:
  0.0 74.8 %layer.1 = bf16[1024,256]{1,0:T(8,128)(2,1)} custom-call(bf16[1024,256]{1,0:T(8,128)(2,1)} %tok_h.1, f32[1,2048]{1,0:T(1,128)} %bitcast.11, bf16[2048,128]{1,0:T(8,128)(2,1)} %wq_h.1, bf16[64,2048]{1,0:T(8,128)(2,1)} %bitcast.6, bf16[64,2048]{1,0:T(8,128)(2,1)} %bitcast.7, bf16[64,2048]{1,0:T(8,128)(2,1)} %bitcast.8, bf16[64,2048]{1,0:T(8,128)(2,1)} %bitcast.9, ...), custom_call_target="tpu_custom_call" | custom-call | tf_op jit(solution)/shard_map/layer/pallas_call | solution.py:470
  74.8 1.9 %copy.17 = bf16[1024,256]{1,0:T(8,128)(2,1)} copy(bf16[1024,256]{1,0:T(8,128)(2,1)} %layer.1) | data formatting | bytes 1048576

commit v3 on v2

--- a/solution.py
+++ b/solution.py
@@ -18,13 +18,14 @@
 BF16 = jnp.bfloat16
 NT = (((1,), (1,)), ((), ()))
 TN = (((0,), (0,)), ((), ()))
+AHEAD = 3
 
 L1, R1, OPP, SIB = 0, 1, 2, 3
 
 
 def kernel(n_sp, nx, tok_h, gain_h, wq_h, wk_h, wv_h, wrq_h, wrk_h, wrv_h, wrg_h, sink_ref, dec_h, init_h, inv_h, oa_h, or_h,
            out_h,
-           X, W1, W2, gain, dec, init, inv, Q, KV, V, G, QR, QB, QX, RL, TT, SL, A, R, WO, OA, OUT,
+           X, W1, W2, gain, dec, init, inv, Q, KV, V, G, SG, COS, SIN, QR, QB, QX, RL, TT, SL, A, R, WO, OA, OUT,
            XS, ZG, ZS, DX, DZ, crow, bl8, pre8,
            lsem, xs_s, xs_r, as_s, as_r, rs_s, rs_r, w1_s, w1_r, w2_s, w2_r, sx_s, sx_r, dx_s, dx_r, sz_s, sz_r, dz_s, dz_r,
            h_s, h_r):
@@ -136,10 +137,10 @@
 
     own, pass_on, pass_last, arrived, sent = gather(X, BLK, xs_s, xs_r)
     a_own, a_pass, a_last, a_arrived, a_sent = gather(A, arows, as_s, as_r)
-    r_own, r_pass, r_last, r_arrived, r_sent = gather(R, arows, rs_s, rs_r)
-
-    own(0)
-    own(1)
+    r_own, r_pass, r_last, r_arrived, r_sent = gather(R, BLK, rs_s, rs_r)
+
+    for k in range(AHEAD):
+        own(k)
     for d in range(1, nx):
         put(DX.at[x], DX.at[x], dx_s.at[d], dx_r.at[d], (z * nx + (x + d) % nx, t)).start()
 
@@ -154,119 +155,66 @@
         row = jnp.broadcast_to(crow[pl.ds(j, 1), :], (BLK, BLK))
         return jnp.sum(jnp.where(lane_b == row_b, row, 0.0), axis=1, keepdims=True)
 
-    def project(j):
+    def tables(j, carry):
         pos = (s * rows + j * BLK + row_b).astype(F32)
         angle = pos * inv[...]
         scale = jnp.where(low, 1.0, 64**-0.5).astype(F32)
-        cosine = jnp.cos(angle) * scale
-        sine = jnp.sin(angle) * jnp.where(lane_b % 64 < 32, -scale, scale)
-        cc = column(j)
-        bl = bl8[pl.ds(j, 1), :]
-        pre = pre8[pl.ds(j, 1), :]
-        arrived(j)
-        squares = jnp.zeros((BLK, cw), F32)
+        COS[blk(j), :] = jnp.cos(angle) * scale
+        SIN[blk(j), :] = jnp.sin(angle) * jnp.where(lane_b % 64 < 32, -scale, scale)
+        return carry
+
+    def project(m):
+        arrived(2 * m)
+        arrived(2 * m + 1)
+        two = pl.ds(pl.multiple_of(m * 2 * BLK, 2 * BLK), 2 * BLK)
+        squares = jnp.zeros((2 * BLK, cw), F32)
         parts = []
         for b in range(8):
-            xf = X[b, blk(j), :].astype(F32)
+            xf = X[b, two, :].astype(F32)
             squares = squares + xf * xf
             parts.append((xf * gain[:, b * cw : (b + 1) * cw]).astype(BF16))
         normed = jnp.concatenate(parts, axis=1)
         inv_rms = lax.rsqrt(jnp.sum(squares, axis=1, keepdims=True) / width + NORM_EPS)
-        p1 = (jnp.dot(normed, W1[...], preferred_element_type=F32) * inv_rms).astype(BF16)
-        p2 = (lax.dot_general(normed, W2[...], NT, preferred_element_type=F32) * inv_rms).astype(BF16)
-        Q[blk(j), :] = p1[:, 0:128]
-        v = p1[:, 128:256]
-        V[blk(j), :] = v
-        G[blk(j), :] = p1[:, 256:384]
-        KV[blk(j + 1), :] = p2[:, 0:128]
-        rqk = p2[:, 128:256].astype(F32)
-        swapped = jnp.where(lane_b % 64 < 32, pltpu.roll(rqk, 96, 1), pltpu.roll(rqk, 32, 1))
-        rot = rqk * cosine + swapped * sine
-        QR[blk(j), :] = rot.astype(BF16)
-        other = pltpu.roll(rot, 64, 1)
-        qq = jnp.where(low, rot, other)
-        kk = jnp.where(low, other, rot)
-        to_end = jnp.exp(bl - cc)
-        to_here = jnp.exp(jnp.broadcast_to(cc, (BLK, BLK)))
-        QB[blk(j), :] = (qq * jnp.where(low, to_here, to_end)).astype(BF16)
-        full = cc + pre
-        QX[blk(j), :] = (qq * jnp.exp(jnp.where(low, full, tot - full))).astype(BF16)
-        kw = (kk * jnp.where(low, to_end, to_here)).astype(BF16)
-        TT[j] = lax.dot_general(kw, v, TN, preferred_element_type=F32)
-
-    for i in range(5, 12):
+        p = (jnp.dot(normed, W1[...], preferred_element_type=F32) * inv_rms).astype(BF16)
+        Q[two, :] = p[:, 0:128]
+        V[two, :] = p[:, 128:256]
+        G[two, :] = p[:, 256:384]
+        KV[pl.ds(pl.multiple_of(m * 2 * BLK + BLK, BLK), 2 * BLK), :] = p[:, 384:512]
+        for h in range(2):
+            j = 2 * m + h
+            cosine, sine, cc = COS[blk(j), :], SIN[blk(j), :], column(j)
+            bl = bl8[pl.ds(j, 1), :]
+            pre = pre8[pl.ds(j, 1), :]
+            rqk = p[h * BLK : (h + 1) * BLK, 512:640].astype(F32)
+            swapped = jnp.where(lane_b % 64 < 32, pltpu.roll(rqk, 96, 1), pltpu.roll(rqk, 32, 1))
+            rot = rqk * cosine + swapped * sine
+            QR[blk(j), :] = rot.astype(BF16)
+            other = pltpu.roll(rot, 64, 1)
+            qq = jnp.where(low, rot, other)
+            kk = jnp.where(low, other, rot)
+            to_end = jnp.exp(bl - cc)
+            to_here = jnp.exp(jnp.broadcast_to(cc, (BLK, BLK)))
+            QB[blk(j), :] = (qq * jnp.where(low, to_here, to_end)).astype(BF16)
+            full = cc + pre
+            QX[blk(j), :] = (qq * jnp.exp(jnp.where(low, full, tot - full))).astype(BF16)
+            kw = (kk * jnp.where(low, to_end, to_here)).astype(BF16)
+            v = p[h * BLK : (h + 1) * BLK, 128:256]
+            TT[j] = lax.dot_general(kw, v, TN, preferred_element_type=F32)
+
+    for i in range(5, 14):
         copies[i].wait()
-
-    def step(k, carry):
-        @pl.when(k < nb - 2)
-        def _():
-            own(k + 2)
-
-        @pl.when(k < nb)
-        def _():
-            pass_on(k)
-
-        @pl.when((k >= 1) & (k < nb + 1))
-        def _():
-            pass_last(k - 1)
-
-        @pl.when(k >= 2)
-        def _():
-            project(k - 2)
-
-        return carry
-
-    lax.fori_loop(0, nb + 2, step, 0)
+    for b in range(8):
+        W1[b * cw : (b + 1) * cw, 384:640] = W2[:, b * cw : (b + 1) * cw].T
+    lax.fori_loop(0, nb, tables, 0)
 
     halo_up = put(KV.at[pl.ds(rows, BLK), :], KV.at[pl.ds(0, BLK), :], h_s.at[0], h_r.at[0], (up, t))
     halo_down = put(KV.at[pl.ds(BLK, BLK), :], KV.at[pl.ds(rows + BLK, BLK), :], h_s.at[1], h_r.at[1], (down, t))
-    halo_up.start()
-    halo_down.start()
-
-    f = jnp.zeros((64, RV), F32)
-    g = jnp.zeros((64, RV), F32)
-    for b in range(nb):
-        SL[b, 0:64, :] = f.astype(BF16)
-        f = jnp.exp(bl8[b : b + 1, :]) * f + TT[b, 0:64, :]
-        e = nb - 1 - b
-        SL[e, 64:128, :] = g.astype(BF16)
-        g = jnp.exp(bl8[e : e + 1, :]) * g + TT[e, 64:128, :]
-    XS[x, 0:64, :] = f.astype(BF16)
-    XS[x, 64:128, :] = g.astype(BF16)
-    for d in range(1, nx):
-        put(XS.at[x], XS.at[x], sx_s.at[d], sx_r.at[d], (z * nx + (x + d) % nx, t)).start()
-    for d in range(1, nx):
-        put(DX.at[(x + nx - d) % nx], DX.at[(x + nx - d) % nx], dx_s.at[d], dx_r.at[d], (s, sib)).wait_recv()
-    total = DX[0]
-    for i in range(1, nx):
-        total = total + DX[i]
-    DZ[z] = total
-    for d in range(1, nz):
-        put(DZ.at[z], DZ.at[z], dz_s.at[d], dz_r.at[d], (((z + d) % nz) * nx + x, t)).start()
-
-    copies[12].wait()
-    copies[13].wait()
-    for d in range(1, 8):
-        to = (t + d) % 8
-        cols = pl.ds(pl.multiple_of(to * ocw, 128), ocw)
-        put(oa_h.at[mine, cols], WO.at[0, t, mine, :], w1_s.at[0, d], w1_r.at[0, d], (s, to)).start()
-        put(or_h.at[mine, cols], WO.at[1, t, mine, :], w1_s.at[1, d], w1_r.at[1, d], (s, to)).start()
 
     row_q = lax.broadcasted_iota(jnp.int32, (2 * BLK, BLK), 0) % BLK
     lane_q = lax.broadcasted_iota(jnp.int32, (2 * BLK, BLK), 1)
     sink = jnp.where(lax.broadcasted_iota(jnp.int32, (2 * BLK, 1), 0) < BLK, sink_ref[0], sink_ref[1])
 
-    def attend(i, carry):
-        j = (i + 2) % nb
-
-        @pl.when(i == nb - 2)
-        def _():
-            halo_up.wait_recv()
-
-        @pl.when(i == nb - 3)
-        def _():
-            halo_down.wait_recv()
-
+    def attend(j):
         q = Q[blk(j), :]
         q2 = jnp.concatenate([q[:, 0:64], q[:, 64:128]], axis=0)
         kv = KV[pl.ds(pl.multiple_of(j * BLK, BLK), 3 * BLK), :]
@@ -283,13 +231,116 @@
         o = jnp.dot(ee, kv[:, 64:128], preferred_element_type=F32) / den
         A[t, blk(j), :] = jnp.concatenate([o[0:BLK], o[BLK : 2 * BLK]], axis=1).astype(BF16)
 
-        @pl.when(i % 2 == 1)
-        def _():
-            a_own(j // 2)
-
-        return carry
-
-    lax.fori_loop(0, nb, attend, 0)
+    def weights_out():
+        for i, half in enumerate((oa_h, or_h)):
+            for d in range(1, 8):
+                to = (t + d) % 8
+                cols = pl.ds(pl.multiple_of(to * ocw, 128), ocw)
+                put(half.at[mine, cols], WO.at[i, t, mine, :], w1_s.at[i, d], w1_r.at[i, d], (s, to)).start()
+
+    def on(k):
+        pass_on(k)
+        if k + AHEAD < nb:
+            own(k + AHEAD)
+
+    on(0)
+    on(1)
+    on(2)
+    pass_last(0)
+    on(3)
+    pass_last(1)
+    on(4)
+    project(0)
+    halo_down.start()
+    pass_last(2)
+    on(5)
+    pass_last(3)
+    on(6)
+    project(1)
+    pass_last(4)
+    on(7)
+    weights_out()
+    pass_last(5)
+    attend(1)
+    attend(2)
+    pass_last(6)
+    project(2)
+    pass_last(7)
+    project(3)
+    halo_up.start()
+
+    f = jnp.zeros((64, RV), F32)
+    g = jnp.zeros((64, RV), F32)
+    for b in range(nb):
+        SL[b, 0:64, :] = f.astype(BF16)
+        f = jnp.exp(bl8[b : b + 1, :]) * f + TT[b, 0:64, :]
+        e = nb - 1 - b
+        SL[e, 64:128, :] = g.astype(BF16)
+        g = jnp.exp(bl8[e : e + 1, :]) * g + TT[e, 64:128, :]
+    XS[x, 0:64, :] = f.astype(BF16)
+    XS[x, 64:128, :] = g.astype(BF16)
+    for d in range(1, nx):
+        put(XS.at[x], XS.at[x], sx_s.at[d], sx_r.at[d], (z * nx + (x + d) % nx, t)).start()
+
+    for d in range(1, nx):
+        o = (x + nx - d) % nx
+        put(DX.at[o], DX.at[o], dx_s.at[d], dx_r.at[d], (s, sib)).wait_recv()
+    total = DX[0]
+    for i in range(1, nx):
+        total = total + DX[i]
+    DZ[z] = total
+    for d in range(1, nz):
+        put(DZ.at[z], DZ.at[z], dz_s.at[d], dz_r.at[d], (((z + d) % nz) * nx + x, t)).start()
+
+    attend(3)
+    attend(4)
+    a_own(1)
+    halo_down.wait_recv()
+    attend(5)
+    attend(6)
+    attend(7)
+    a_own(2)
+    a_own(3)
+
+    xr, xl = z * nx + (x + 1) % nx, z * nx + (x + nx - 1) % nx
+
+    def quarter_of(o):
+        return pl.ds(pl.multiple_of(((x + o + nx) % nx) * quarter, quarter), quarter)
+
+    def w2_own(i):
+        for d in range(1, 8):
+            ref = WO.at[i, (t + 8 - d) % 8, mine, :]
+            put(ref, ref, w1_s.at[i, d], w1_r.at[i, d], (s, sib)).wait_recv()
+        ref = WO.at[i, :, mine, :]
+        put(ref, ref, w2_s.at[i, 0], w2_r.at[i, 0], (xr, t)).start()
+        put(ref, ref, w2_s.at[i, 1], w2_r.at[i, 1], (xl, t)).start()
+
+    def w2_pass(i):
+        from_left = WO.at[i, :, quarter_of(-1), :]
+        from_right = WO.at[i, :, quarter_of(1), :]
+        put(from_left, from_left, w2_s.at[i, 0], w2_r.at[i, 0], (xr, t)).wait_recv()
+        half = WO.at[i, 0:4, quarter_of(-1), :]
+        put(half, half, w2_s.at[i, 2], w2_r.at[i, 2], (xr, t)).start()
+        put(from_right, from_right, w2_s.at[i, 1], w2_r.at[i, 1], (xl, t)).wait_recv()
+        half = WO.at[i, 4:8, quarter_of(1), :]
+        put(half, half, w2_s.at[i, 3], w2_r.at[i, 3], (xl, t)).start()
+
+    def w2_done(i):
+        half = WO.at[i, 0:4, quarter_of(2), :]
+        put(half, half, w2_s.at[i, 2], w2_r.at[i, 2], (xr, t)).wait_recv()
+        half = WO.at[i, 4:8, quarter_of(2), :]
+        put(half, half, w2_s.at[i, 3], w2_r.at[i, 3], (xl, t)).wait_recv()
+
+    def w2_sent(i):
+        ref = WO.at[i, :, mine, :]
+        half = WO.at[i, 0:4, mine, :]
+        put(ref, ref, w2_s.at[i, 0], w2_r.at[i, 0], (xr, t)).wait_send()
+        put(ref, ref, w2_s.at[i, 1], w2_r.at[i, 1], (xl, t)).wait_send()
+        put(half, half, w2_s.at[i, 2], w2_r.at[i, 2], (xr, t)).wait_send()
+        put(half, half, w2_s.at[i, 3], w2_r.at[i, 3], (xl, t)).wait_send()
+
+    w2_own(0)
+    w2_own(1)
 
     for d in range(1, nx):
         o = (x + nx - d) % nx
@@ -317,11 +368,11 @@
     for d in range(1, nz):
         put(ZG.at[(z + d) // nz], ZS.at[z], sz_s.at[d], sz_r.at[d], (((z + d) % nz) * nx + x, t)).start()
 
-    a_order = [(i + 1) % na for i in range(na)]
-    for k in a_order:
-        a_pass(k)
-
-    def inside(j, carry):
+    halo_up.wait_recv()
+    attend(0)
+    a_own(0)
+
+    def inside(j):
         cc = column(j)
         cr = crow[pl.ds(j, 1), :]
         qk = QR[blk(j), :]
@@ -330,21 +381,24 @@
         RL[blk(j), :] = jnp.dot(w, V[blk(j), :], preferred_element_type=F32) + jnp.dot(
             QB[blk(j), :], SL[j], preferred_element_type=F32
         )
+        gate = G[blk(j), :].astype(F32)
+        SG[blk(j), :] = gate / (1.0 + jnp.exp(-gate))
+
+    def inside_two(m, carry):
+        inside(2 * m)
+        inside(2 * m + 1)
         return carry
 
-    lax.fori_loop(0, nb, inside, 0)
-
-    for d in range(1, 8):
-        fr = (t + 8 - d) % 8
-        for i in range(2):
-            ref = WO.at[i, fr, mine, :]
-            put(ref, ref, w1_s.at[i, d], w1_r.at[i, d], (s, sib)).wait_recv()
-    for d in range(1, nx):
-        ref = WO.at[:, :, mine, :]
-        put(ref, ref, w2_s.at[d], w2_r.at[d], (z * nx + (x + d) % nx, t)).start()
-
-    for k in a_order:
+    lax.fori_loop(0, na, inside_two, 0)
+
+    for k in range(1, na):
+        a_pass(k)
+
+    w2_pass(0)
+    for k in range(1, na):
         a_last(k)
+    w2_pass(1)
+    a_pass(0)
 
     for d in range(1, nz):
         o = (z + nz - d) % nz
@@ -360,68 +414,64 @@
         gz = jnp.where(o > z, jnp.exp(DZ[o][0:1, :]) * gz + term, gz)
     ST = jnp.concatenate([fx + jnp.exp(dfx) * fz, gx + jnp.exp(dgx) * gz], axis=0).astype(BF16)
 
-    def finish(j, carry):
-        ret = RL[blk(j), :] + jnp.dot(QX[blk(j), :], carry, preferred_element_type=F32)
+    def big(k):
+        return pl.ds(pl.multiple_of(k * arows, arows), arows)
+
+    def finish(k, carry):
+        ret = RL[big(k), :] + jnp.dot(QX[big(k), :], carry, preferred_element_type=F32)
         cen = ret - jnp.mean(ret, axis=1, keepdims=True)
         nrm = cen * lax.rsqrt(jnp.mean(cen * cen, axis=1, keepdims=True) + NORM_EPS)
-        gate = G[blk(j), :].astype(F32)
-        R[t, blk(j), :] = (gate / (1.0 + jnp.exp(-gate)) * nrm).astype(BF16)
-
-        @pl.when(j % 2 == 1)
-        def _():
-            r_own(j // 2)
-
+        R[t, big(k), :] = (SG[big(k), :] * nrm).astype(BF16)
+        r_own(2 * k)
+        r_own(2 * k + 1)
         return carry
 
-    lax.fori_loop(0, nb, finish, ST)
-
-    for k in range(na):
-        r_pass(k)
-
-    for k in range(na):
-        a_arrived(k)
-    for d in range(1, nx):
-        ref = WO.at[:, :, pl.ds(pl.multiple_of(((x + nx - d) % nx) * quarter, quarter), quarter), :]
-        put(ref, ref, w2_s.at[d], w2_r.at[d], (s, sib)).wait_recv()
-
-    def big(k):
-        return pl.ds(pl.multiple_of(k * arows, arows), arows)
-
-    def out_att(k, carry):
+    lax.fori_loop(0, na, finish, ST)
+
+    def out_att(k):
         lhs = jnp.concatenate([A[b, big(k), :] for b in range(8)], axis=1)
         OA[big(k), :] = jnp.dot(lhs, WO[0].reshape(8 * BLK, ocw), preferred_element_type=F32)
-        return carry
-
-    lax.fori_loop(0, na, out_att, 0)
-
-    for k in range(na):
-        r_last(k)
 
     def out_ret(k, carry):
         r_arrived(k)
-        lhs = jnp.concatenate([R[b, big(k), :] for b in range(8)], axis=1)
-        acc = OA[big(k), :] + jnp.dot(lhs, WO[1].reshape(8 * BLK, ocw), preferred_element_type=F32)
-        OUT[big(k), :] = acc.astype(BF16)
-        pltpu.make_async_copy(OUT.at[big(k), :], out_h.at[big(k), :], lsem.at[14 + k]).start()
+        lhs = jnp.concatenate([R[b, blk(k), :] for b in range(8)], axis=1)
+        acc = OA[blk(k), :] + jnp.dot(lhs, WO[1].reshape(8 * BLK, ocw), preferred_element_type=F32)
+        OUT[blk(k), :] = acc.astype(BF16)
+        pltpu.make_async_copy(OUT.at[blk(k), :], out_h.at[blk(k), :], lsem.at[14 + k]).start()
         return carry
 
-    lax.fori_loop(0, na, out_ret, 0)
+    for k in range(nb):
+        r_pass(k)
+        if k == 1:
+            a_last(0)
+        if k == nb // 2:
+            for i in range(na):
+                a_arrived(i)
+            w2_done(0)
+        if k >= nb // 2:
+            out_att(k - nb // 2)
+    for k in range(nb // 2):
+        r_last(k)
+    w2_done(1)
+    for k in range(nb // 2, nb):
+        out_ret(k - nb // 2, 0)
+        r_last(k)
+    lax.fori_loop(nb // 2, nb, out_ret, 0)
 
     def drain(k, carry):
         sent(k)
+        r_sent(k)
+        pltpu.make_async_copy(OUT.at[blk(k), :], out_h.at[blk(k), :], lsem.at[14 + k]).wait()
         return carry
 
     lax.fori_loop(0, nb, drain, 0)
     for k in range(na):
         a_sent(k)
-        r_sent(k)
-        pltpu.make_async_copy(OUT.at[big(k), :], out_h.at[big(k), :], lsem.at[14 + k]).wait()
-    for d in range(1, 8):
-        for i in range(2):
+    for i in range(2):
+        for d in range(1, 8):
             put(oa_h.at[mine, my_cols], WO.at[i, t, mine, :], w1_s.at[i, d], w1_r.at[i, d], (s, sib)).wait_send()
+        w2_sent(i)
     for d in range(1, nx):
-        ref = WO.at[:, :, mine, :]
-        put(ref, ref, w2_s.at[d], w2_r.at[d], (s, sib)).wait_send()
         put(XS.at[x], XS.at[x], sx_s.at[d], sx_r.at[d], (s, sib)).wait_send()
         put(DX.at[x], DX.at[x], dx_s.at[d], dx_r.at[d], (s, sib)).wait_send()
     for d in range(1, nz):
@@ -437,7 +487,7 @@
     width = 8 * cw
     ocw = out_att.shape[1] // 8
     nb, na = rows // BLK, rows // (2 * BLK)
-    nx = 4 if n_sp >= 16 else 2
+    nx = 4
     nz = n_sp // nx
     inverse = (np.float64(ROPE_BASE) ** (-2.0 * (np.arange(128) % 32) / 64)).astype(np.float32)[None, :]
     dma = pltpu.SemaphoreType.DMA
@@ -446,16 +496,16 @@
     specs[9] = pl.BlockSpec(memory_space=pltpu.SMEM)
     vm = pltpu.VMEM
     scratch = [
-        vm((8, rows, cw), BF16), vm((width, 384), BF16), vm((256, width), BF16), vm((1, width), F32), vm((1, rows), F32),
+        vm((8, rows, cw), BF16), vm((width, 640), BF16), vm((256, width), BF16), vm((1, width), F32), vm((1, rows), F32),
         vm((128, 128), F32), vm((1, 128), F32),
-        vm((rows, 128), BF16), vm((rows + 2 * BLK, 128), BF16), vm((rows, 128), BF16), vm((rows, 128), BF16),
-        vm((rows, 128), BF16), vm((rows, 128), BF16), vm((rows, 128), BF16), vm((rows, 128), F32),
+        vm((rows, 128), BF16), vm((rows + 2 * BLK, 128), BF16), vm((rows, 128), BF16), vm((rows, 128), BF16), vm((rows, 128), F32),
+        vm((rows, 128), F32), vm((rows, 128), F32), vm((rows, 128), BF16), vm((rows, 128), BF16), vm((rows, 128), BF16), vm((rows, 128), F32),
         vm((nb, 128, 128), F32), vm((nb, 128, 128), BF16),
         vm((8, rows, 128), BF16), vm((8, rows, 128), BF16), vm((2, 8, 128, ocw), BF16), vm((rows, ocw), F32), vm((rows, ocw), BF16),
         vm((nx, 128, 128), BF16), vm((2, 64, 128), BF16), vm((nz, 64, 128), BF16), vm((nx, 8, 128), F32), vm((nz, 8, 128), F32),
         vm((nb, 128), F32), vm((nb, 128), F32), vm((nb, 128), F32),
-        dma((14 + na,)), dma((7, nb)), dma((7, nb)), dma((7, na)), dma((7, na)), dma((7, na)), dma((7, na)),
-        dma((2, 8)), dma((2, 8)), dma((nx,)), dma((nx,)), dma((nx,)), dma((nx,)), dma((nx,)), dma((nx,)),
+        dma((14 + nb,)), dma((7, nb)), dma((7, nb)), dma((7, na)), dma((7, na)), dma((7, nb)), dma((7, nb)),
+        dma((2, 8)), dma((2, 8)), dma((2, 4)), dma((2, 4)), dma((nx,)), dma((nx,)), dma((nx,)), dma((nx,)),
         dma((max(nz, 2),)), dma((max(nz, 2),)), dma((max(nz, 2),)), dma((max(nz, 2),)), dma((2,)), dma((2,)),
     ]
     call = pl.pallas_call(

time: 76.8 us -> 68.5 us (0.89)
  Pallas kernels: 74.8 us -> 66.4 us
    pallas_call x1, Pallas kernels: 74.8 us -> 66.4 us  [body(): call(tokens, norm_gain.reshape(1, width), att_query, att_key.T, att_value...]
where the time goes in v3:
time: 68.5 us; the launch traced here: 68.3 us
  Pallas kernels  66.4 us (97%)
  local copies, waits for them, and re-layouts  1.87 us (3%)
    pallas_call x1, Pallas kernels, body(): call(tokens, norm_gain.reshape(1, width), att_query, att_key.T, att_value...  66.4 us
    unnamed x1, local copies, waits for them, and re-layouts  1.87 us

profile of v3, /device:TPU:1, one launch (start us, length us, event | category | flops | bytes accessed | tf_op | source)
XLA Modules:
  0.0 68.3 jit_solution(5689376404686499477)
XLA Ops:
  0.0 66.4 %layer.1 = bf16[1024,256]{1,0:T(8,128)(2,1)} custom-call(bf16[1024,256]{1,0:T(8,128)(2,1)} %tok_h.1, f32[1,2048]{1,0:T(1,128)} %bitcast.11, bf16[2048,128]{1,0:T(8,128)(2,1)} %wq_h.1, bf16[64,2048]{1,0:T(8,128)(2,1)} %bitcast.6, bf16[64,2048]{1,0:T(8,128)(2,1)} %bitcast.7, bf16[64,2048]{1,0:T(8,128)(2,1)} %bitcast.8, bf16[64,2048]{1,0:T(8,128)(2,1)} %bitcast.9, ...), custom_call_target="tpu_custom_call" | custom-call | tf_op jit(solution)/shard_map/layer/pallas_call | solution.py:520
  66.5 1.9 %copy.17 = bf16[1024,256]{1,0:T(8,128)(2,1)} copy(bf16[1024,256]{1,0:T(8,128)(2,1)} %layer.1) | data formatting | bytes 1048576

commit v4 on v3

--- a/solution.py
+++ b/solution.py
@@ -18,14 +18,14 @@
 BF16 = jnp.bfloat16
 NT = (((1,), (1,)), ((), ()))
 TN = (((0,), (0,)), ((), ()))
-AHEAD = 3
+AHEAD = 5
 
 L1, R1, OPP, SIB = 0, 1, 2, 3
 
 
 def kernel(n_sp, nx, tok_h, gain_h, wq_h, wk_h, wv_h, wrq_h, wrk_h, wrv_h, wrg_h, sink_ref, dec_h, init_h, inv_h, oa_h, or_h,
            out_h,
-           X, W1, W2, gain, dec, init, inv, Q, KV, V, G, SG, COS, SIN, QR, QB, QX, RL, TT, SL, A, R, WO, OA, OUT,
+           X, W1, W2, gain, dec, init, inv, Q, KV, V, G, SG, COS, SIN, ACC, SQ, QR, QB, QX, RL, TT, SL, A, R, WO, OA, OUT,
            XS, ZG, ZS, DX, DZ, crow, bl8, pre8,
            lsem, xs_s, xs_r, as_s, as_r, rs_s, rs_r, w1_s, w1_r, w2_s, w2_r, sx_s, sx_r, dx_s, dx_r, sz_s, sz_r, dz_s, dz_r,
            h_s, h_r):
@@ -44,6 +44,9 @@
     left = 2 * ((y + 3) % 4) + c
     opp = 2 * ((y + 2) % 4) + c
     sib = 2 * y + (1 - c)
+    sib_right = 2 * ((y + 1) % 4) + 1 - c
+    sib_left = 2 * ((y + 3) % 4) + 1 - c
+    sib_opp = 2 * ((y + 2) % 4) + 1 - c
     up, down = (s + 1) % n_sp, (s + n_sp - 1) % n_sp
 
     loads = [
@@ -123,21 +126,27 @@
             hop(opp, k, 5, OPP, right).wait_recv()
             hop(opp, k, 5, SIB + 3, sib).start()
 
+        def arrived_near(k):
+            hop(sib, k, 2, SIB, sib).wait_recv()
+            hop(sib_left, k, 3, SIB + 1, sib).wait_recv()
+            hop(sib_right, k, 4, SIB + 2, sib).wait_recv()
+
+        def arrived_opp(k):
+            hop(sib_opp, k, 5, SIB + 3, sib).wait_recv()
+
         def arrived(k):
-            hop(sib, k, 2, SIB, sib).wait_recv()
-            hop(2 * ((y + 3) % 4) + 1 - c, k, 3, SIB + 1, sib).wait_recv()
-            hop(2 * ((y + 1) % 4) + 1 - c, k, 4, SIB + 2, sib).wait_recv()
-            hop(2 * ((y + 2) % 4) + 1 - c, k, 5, SIB + 3, sib).wait_recv()
+            arrived_near(k)
+            arrived_opp(k)
 
         def sent(k):
             for i in range(7):
                 hop(t, k, i, L1, right).wait_send()
 
-        return own, pass_on, pass_last, arrived, sent
-
-    own, pass_on, pass_last, arrived, sent = gather(X, BLK, xs_s, xs_r)
-    a_own, a_pass, a_last, a_arrived, a_sent = gather(A, arows, as_s, as_r)
-    r_own, r_pass, r_last, r_arrived, r_sent = gather(R, BLK, rs_s, rs_r)
+        return own, pass_on, pass_last, arrived, sent, arrived_near, arrived_opp
+
+    own, pass_on, pass_last, arrived, sent, arrived_near, arrived_opp = gather(X, BLK, xs_s, xs_r)
+    a_own, a_pass, a_last, a_arrived, a_sent, _, _ = gather(A, arows, as_s, as_r)
+    r_own, r_pass, r_last, r_arrived, r_sent, _, _ = gather(R, BLK, rs_s, rs_r)
 
     for k in range(AHEAD):
         own(k)
@@ -163,19 +172,31 @@
         SIN[blk(j), :] = jnp.sin(angle) * jnp.where(lane_b % 64 < 32, -scale, scale)
         return carry
 
+    def pair(m):
+        return pl.ds(pl.multiple_of(m * 2 * BLK, 2 * BLK), 2 * BLK)
+
+    def sums(m, acc, squares, blocks):
+        for b in blocks:
+            cols = pl.ds(pl.multiple_of(b * cw, cw), cw)
+            xf = X[b, pair(m), :].astype(F32)
+            sq = xf * xf
+            squares = squares + sum(sq[:, i : i + 128] for i in range(0, cw, 128))
+            acc = acc + jnp.dot((xf * gain[:, cols]).astype(BF16), W1[cols, :], preferred_element_type=F32)
+        return acc, squares
+
+    def project_near(m):
+        arrived_near(2 * m)
+        arrived_near(2 * m + 1)
+        zero = jnp.zeros((2 * BLK, 640), F32), jnp.zeros((2 * BLK, 128), F32)
+        ACC[m % 2], SQ[m % 2] = sums(m, *zero, (t, sib, left, right, sib_left, sib_right))
+
     def project(m):
-        arrived(2 * m)
-        arrived(2 * m + 1)
-        two = pl.ds(pl.multiple_of(m * 2 * BLK, 2 * BLK), 2 * BLK)
-        squares = jnp.zeros((2 * BLK, cw), F32)
-        parts = []
-        for b in range(8):
-            xf = X[b, two, :].astype(F32)
-            squares = squares + xf * xf
-            parts.append((xf * gain[:, b * cw : (b + 1) * cw]).astype(BF16))
-        normed = jnp.concatenate(parts, axis=1)
+        two = pair(m)
+        arrived_opp(2 * m)
+        arrived_opp(2 * m + 1)
+        acc, squares = sums(m, ACC[m % 2], SQ[m % 2], (opp, sib_opp))
         inv_rms = lax.rsqrt(jnp.sum(squares, axis=1, keepdims=True) / width + NORM_EPS)
-        p = (jnp.dot(normed, W1[...], preferred_element_type=F32) * inv_rms).astype(BF16)
+        p = (acc * inv_rms).astype(BF16)
         Q[two, :] = p[:, 0:128]
         V[two, :] = p[:, 128:256]
         G[two, :] = p[:, 256:384]
@@ -246,26 +267,32 @@
     on(0)
     on(1)
     on(2)
+    on(3)
+    project_near(0)
+    on(4)
+    project_near(1)
     pass_last(0)
-    on(3)
+    on(5)
     pass_last(1)
-    on(4)
+    on(6)
     project(0)
     halo_down.start()
     pass_last(2)
-    on(5)
+    on(7)
+    weights_out()
     pass_last(3)
-    on(6)
+    project_near(2)
     project(1)
     pass_last(4)
-    on(7)
-    weights_out()
     pass_last(5)
+    project_near(3)
     attend(1)
-    attend(2)
     pass_last(6)
     project(2)
     pass_last(7)
+    attend(2)
+    attend(3)
+    a_own(1)
     project(3)
     halo_up.start()
 
@@ -292,14 +319,12 @@
     for d in range(1, nz):
         put(DZ.at[z], DZ.at[z], dz_s.at[d], dz_r.at[d], (((z + d) % nz) * nx + x, t)).start()
 
-    attend(3)
     attend(4)
-    a_own(1)
+    attend(5)
+    a_own(2)
     halo_down.wait_recv()
-    attend(5)
     attend(6)
     attend(7)
-    a_own(2)
     a_own(3)
 
     xr, xl = z * nx + (x + 1) % nx, z * nx + (x + nx - 1) % nx
@@ -341,6 +366,27 @@
 
     w2_own(0)
     w2_own(1)
+
+    def inside(j):
+        cc = column(j)
+        cr = crow[pl.ds(j, 1), :]
+        qk = QR[blk(j), :]
+        sc = lax.dot_general(qk[:, 0:64], qk[:, 64:128], NT, preferred_element_type=F32)
+        w = (sc * jnp.exp(-jnp.abs(cc - cr))).astype(BF16)
+        RL[blk(j), :] = jnp.dot(w, V[blk(j), :], preferred_element_type=F32) + jnp.dot(
+            QB[blk(j), :], SL[j], preferred_element_type=F32
+        )
+        gate = G[blk(j), :].astype(F32)
+        SG[blk(j), :] = gate / (1.0 + jnp.exp(-gate))
+
+    def inside_two(m, carry):
+        inside(2 * m)
+        inside(2 * m + 1)
+        return carry
+
+    lax.fori_loop(0, na, inside_two, 0)
+
+    a_pass(1)
 
     for d in range(1, nx):
         o = (x + nx - d) % nx
@@ -372,33 +418,29 @@
     attend(0)
     a_own(0)
 
-    def inside(j):
-        cc = column(j)
-        cr = crow[pl.ds(j, 1), :]
-        qk = QR[blk(j), :]
-        sc = lax.dot_general(qk[:, 0:64], qk[:, 64:128], NT, preferred_element_type=F32)
-        w = (sc * jnp.exp(-jnp.abs(cc - cr))).astype(BF16)
-        RL[blk(j), :] = jnp.dot(w, V[blk(j), :], preferred_element_type=F32) + jnp.dot(
-            QB[blk(j), :], SL[j], preferred_element_type=F32
-        )
-        gate = G[blk(j), :].astype(F32)
-        SG[blk(j), :] = gate / (1.0 + jnp.exp(-gate))
-
-    def inside_two(m, carry):
-        inside(2 * m)
-        inside(2 * m + 1)
+    for k in range(2, na):
+        a_pass(k)
+
+    def drain(k, carry):
+        sent(k)
         return carry
 
-    lax.fori_loop(0, na, inside_two, 0)
-
-    for k in range(1, na):
-        a_pass(k)
-
+    lax.fori_loop(0, nb, drain, 0)
+    for i in range(2):
+        for d in range(1, 8):
+            put(oa_h.at[mine, my_cols], WO.at[i, t, mine, :], w1_s.at[i, d], w1_r.at[i, d], (s, sib)).wait_send()
+    for d in range(1, nx):
+        put(XS.at[x], XS.at[x], sx_s.at[d], sx_r.at[d], (s, sib)).wait_send()
+        put(DX.at[x], DX.at[x], dx_s.at[d], dx_r.at[d], (s, sib)).wait_send()
+    halo_up.wait_send()
+    halo_down.wait_send()
+
+    a_last(1)
     w2_pass(0)
-    for k in range(1, na):
-        a_last(k)
+    a_last(2)
+    a_last(3)
+    a_pass(0)
     w2_pass(1)
-    a_pass(0)
 
     for d in range(1, nz):
         o = (z + nz - d) % nz
@@ -432,53 +474,49 @@
         lhs = jnp.concatenate([A[b, big(k), :] for b in range(8)], axis=1)
         OA[big(k), :] = jnp.dot(lhs, WO[0].reshape(8 * BLK, ocw), preferred_element_type=F32)
 
-    def out_ret(k, carry):
-        r_arrived(k)
-        lhs = jnp.concatenate([R[b, blk(k), :] for b in range(8)], axis=1)
-        acc = OA[blk(k), :] + jnp.dot(lhs, WO[1].reshape(8 * BLK, ocw), preferred_element_type=F32)
-        OUT[blk(k), :] = acc.astype(BF16)
-        pltpu.make_async_copy(OUT.at[blk(k), :], out_h.at[blk(k), :], lsem.at[14 + k]).start()
-        return carry
-
+    def out_ret(k):
+        r_arrived(2 * k)
+        r_arrived(2 * k + 1)
+        lhs = jnp.concatenate([R[b, big(k), :] for b in range(8)], axis=1)
+        acc = OA[big(k), :] + jnp.dot(lhs, WO[1].reshape(8 * BLK, ocw), preferred_element_type=F32)
+        OUT[big(k), :] = acc.astype(BF16)
+        pltpu.make_async_copy(OUT.at[big(k), :], out_h.at[big(k), :], lsem.at[14 + k]).start()
+
+    w2_done(0)
+    for k in range(1, na):
+        a_arrived(k)
+        out_att(k)
     for k in range(nb):
         r_pass(k)
         if k == 1:
             a_last(0)
-        if k == nb // 2:
-            for i in range(na):
-                a_arrived(i)
-            w2_done(0)
-        if k >= nb // 2:
-            out_att(k - nb // 2)
+    a_arrived(0)
+    out_att(0)
     for k in range(nb // 2):
         r_last(k)
     w2_done(1)
-    for k in range(nb // 2, nb):
-        out_ret(k - nb // 2, 0)
-        r_last(k)
-    lax.fori_loop(nb // 2, nb, out_ret, 0)
-
-    def drain(k, carry):
-        sent(k)
-        r_sent(k)
-        pltpu.make_async_copy(OUT.at[blk(k), :], out_h.at[blk(k), :], lsem.at[14 + k]).wait()
-        return carry
-
-    lax.fori_loop(0, nb, drain, 0)
     for k in range(na):
         a_sent(k)
     for i in range(2):
-        for d in range(1, 8):
-            put(oa_h.at[mine, my_cols], WO.at[i, t, mine, :], w1_s.at[i, d], w1_r.at[i, d], (s, sib)).wait_send()
         w2_sent(i)
-    for d in range(1, nx):
-        put(XS.at[x], XS.at[x], sx_s.at[d], sx_r.at[d], (s, sib)).wait_send()
-        put(DX.at[x], DX.at[x], dx_s.at[d], dx_r.at[d], (s, sib)).wait_send()
     for d in range(1, nz):
         put(ZG.at[0], ZS.at[z], sz_s.at[d], sz_r.at[d], (s, sib)).wait_send()
         put(DZ.at[z], DZ.at[z], dz_s.at[d], dz_r.at[d], (s, sib)).wait_send()
-    halo_up.wait_send()
-    halo_down.wait_send()
+    out_ret(0)
+    r_last(4)
+    r_last(5)
+    out_ret(1)
+    r_last(6)
+    r_last(7)
+    out_ret(2)
+    for k in range(nb // 2):
+        r_sent(k)
+    out_ret(3)
+
+    for k in range(nb // 2, nb):
+        r_sent(k)
+    for k in range(na):
+        pltpu.make_async_copy(OUT.at[big(k), :], out_h.at[big(k), :], lsem.at[14 + k]).wait()
 
 
 def body(tokens, norm_gain, att_query, att_key, att_value, ret_query, ret_key, ret_value, ret_gate, att_sink, decay_log, init_state,
@@ -499,7 +537,7 @@
         vm((8, rows, cw), BF16), vm((width, 640), BF16), vm((256, width), BF16), vm((1, width), F32), vm((1, rows), F32),
         vm((128, 128), F32), vm((1, 128), F32),
         vm((rows, 128), BF16), vm((rows + 2 * BLK, 128), BF16), vm((rows, 128), BF16), vm((rows, 128), BF16), vm((rows, 128), F32),
-        vm((rows, 128), F32), vm((rows, 128), F32), vm((rows, 128), BF16), vm((rows, 128), BF16), vm((rows, 128), BF16), vm((rows, 128), F32),
+        vm((rows, 128), F32), vm((rows, 128), F32), vm((2, 2 * BLK, 640), F32), vm((2, 2 * BLK, 128), F32), vm((rows, 128), BF16), vm((rows, 128), BF16), vm((rows, 128), BF16), vm((rows, 128), F32),
         vm((nb, 128, 128), F32), vm((nb, 128, 128), BF16),
         vm((8, rows, 128), BF16), vm((8, rows, 128), BF16), vm((2, 8, 128, ocw), BF16), vm((rows, ocw), F32), vm((rows, ocw), BF16),
         vm((nx, 128, 128), BF16), vm((2, 64, 128), BF16), vm((nz, 64, 128), BF16), vm((nx, 8, 128), F32), vm((nz, 8, 128), F32),

time: 68.5 us -> 65.6 us (0.958)
  Pallas kernels: 66.4 us -> 63.6 us
    pallas_call x1, Pallas kernels: 66.4 us -> 63.6 us  [body(): call(tokens, norm_gain.reshape(1, width), att_query, att_key.T, att_value...]
where the time goes in v4:
time: 65.6 us; the launch traced here: 65.5 us
  Pallas kernels  63.6 us (97%)
  local copies, waits for them, and re-layouts  1.87 us (3%)
    pallas_call x1, Pallas kernels, body(): call(tokens, norm_gain.reshape(1, width), att_query, att_key.T, att_value...  63.6 us
    unnamed x1, local copies, waits for them, and re-layouts  1.87 us

profile of v4, /device:TPU:1, one launch (start us, length us, event | category | flops | bytes accessed | tf_op | source)
XLA Modules:
  0.0 65.5 jit_solution(17999381249716190853)
XLA Ops:
  0.0 63.6 %layer.1 = bf16[1024,256]{1,0:T(8,128)(2,1)} custom-call(bf16[1024,256]{1,0:T(8,128)(2,1)} %tok_h.1, f32[1,2048]{1,0:T(1,128)} %bitcast.11, bf16[2048,128]{1,0:T(8,128)(2,1)} %wq_h.1, bf16[64,2048]{1,0:T(8,128)(2,1)} %bitcast.6, bf16[64,2048]{1,0:T(8,128)(2,1)} %bitcast.7, bf16[64,2048]{1,0:T(8,128)(2,1)} %bitcast.8, bf16[64,2048]{1,0:T(8,128)(2,1)} %bitcast.9, ...), custom_call_target="tpu_custom_call" | custom-call | tf_op jit(solution)/shard_map/layer/pallas_call | solution.py:558
  63.6 1.9 %copy.17 = bf16[1024,256]{1,0:T(8,128)(2,1)} copy(bf16[1024,256]{1,0:T(8,128)(2,1)} %layer.1) | data formatting | bytes 1048576

commit v5 on v4

--- a/solution.py
+++ b/solution.py
@@ -27,7 +27,7 @@
            out_h,
            X, W1, W2, gain, dec, init, inv, Q, KV, V, G, SG, COS, SIN, ACC, SQ, QR, QB, QX, RL, TT, SL, A, R, WO, OA, OUT,
            XS, ZG, ZS, DX, DZ, crow, bl8, pre8,
-           lsem, xs_s, xs_r, as_s, as_r, rs_s, rs_r, w1_s, w1_r, w2_s, w2_r, sx_s, sx_r, dx_s, dx_r, sz_s, sz_r, dz_s, dz_r,
+           lsem, xs_s, xs_r, xn_r, xf_r, as_s, as_r, an_r, af_r, rs_s, rs_r, rn_r, rf_r, w1_s, w1_r, w2_s, w2_r, sx_s, sx_r, dx_s, dx_r, sz_s, sz_r, dz_s, dz_r,
            h_s, h_r):
     rows, cw = tok_h.shape
     nb = rows // BLK
@@ -65,9 +65,17 @@
     partners = [(s, (t + d) % 8) for d in range(1, 8)]
     partners += [(z * nx + (x + d) % nx, t) for d in range(1, nx)]
     partners += [(((z + d) % nz) * nx + x, t) for d in range(1, nz)]
-    partners += [(up, t), (down, t)]
-    for p in partners:
+    has_up, has_down = 1 - (s + 1) // n_sp, (s + n_sp - 1) // n_sp
+    for p in reversed(partners):
         pl.semaphore_signal(barrier, inc=1, device_id=p, device_id_type=MESH)
+
+    @pl.when(has_up == 1)
+    def _():
+        pl.semaphore_signal(barrier, inc=1, device_id=(up, t), device_id_type=MESH)
+
+    @pl.when(has_down == 1)
+    def _():
+        pl.semaphore_signal(barrier, inc=1, device_id=(down, t), device_id_type=MESH)
 
     copies[0].wait()
     for b in range(nb):
@@ -87,71 +95,65 @@
     for i in range(1, 5):
         copies[i].wait()
 
-    pl.semaphore_wait(barrier, len(partners))
+    pl.semaphore_wait(barrier, len(partners) + has_up + has_down)
 
     def put(src, dst, send, recv, dev):
         return pltpu.make_async_remote_copy(src_ref=src, dst_ref=dst, send_sem=send, recv_sem=recv, device_id=dev, device_id_type=MESH)
 
-    def gather(buf, n_rows, ss, rs):
+    def gather(buf, n_rows, ss, rs, near, far):
+        group = 2 * BLK // n_rows
+
         def part(b, k):
             return buf.at[b, pl.ds(pl.multiple_of(k * n_rows, n_rows), n_rows), :]
 
         def hop(b, k, send, recv, tp):
             ref = part(b, k)
-            return put(ref, ref, ss.at[send, k], rs.at[recv, k], (s, tp))
+            return put(ref, ref, ss.at[send], recv, (s, tp))
 
         def own(k):
-            hop(t, k, 0, L1, right).start()
-            hop(t, k, 1, R1, left).start()
-            hop(t, k, 2, SIB, sib).start()
+            hop(t, k, 0, rs.at[L1, k], right).start()
+            hop(t, k, 1, rs.at[R1, k], left).start()
+            hop(t, k, 2, near.at[k // group], sib).start()
 
         def pass_on(k):
-            hop(left, k, 3, L1, right).wait_recv()
-            even = k % 2 == 0
-
-            @pl.when(even)
-            def _():
-                hop(left, k, 6, OPP, right).start()
-
-            hop(left, k, 3, SIB + 1, sib).start()
-            hop(right, k, 4, R1, left).wait_recv()
-
-            @pl.when(k % 2 == 1)
-            def _():
-                hop(right, k, 6, OPP, left).start()
-
-            hop(right, k, 4, SIB + 2, sib).start()
+            hop(left, k, 3, rs.at[L1, k], right).wait_recv()
+            if k % 2 == 0:
+                hop(left, k, 6, rs.at[OPP, k], right).start()
+            hop(left, k, 3, near.at[k // group], sib).start()
+            hop(right, k, 4, rs.at[R1, k], left).wait_recv()
+            if k % 2 == 1:
+                hop(right, k, 6, rs.at[OPP, k], left).start()
+            hop(right, k, 4, near.at[k // group], sib).start()
 
         def pass_last(k):
-            hop(opp, k, 5, OPP, right).wait_recv()
-            hop(opp, k, 5, SIB + 3, sib).start()
-
-        def arrived_near(k):
-            hop(sib, k, 2, SIB, sib).wait_recv()
-            hop(sib_left, k, 3, SIB + 1, sib).wait_recv()
-            hop(sib_right, k, 4, SIB + 2, sib).wait_recv()
-
-        def arrived_opp(k):
-            hop(sib_opp, k, 5, SIB + 3, sib).wait_recv()
-
-        def arrived(k):
-            arrived_near(k)
-            arrived_opp(k)
-
-        def sent(k):
+            hop(opp, k, 5, rs.at[OPP, k], right).wait_recv()
+            hop(opp, k, 5, far.at[k // group], sib).start()
+
+        def two(first, blocks, m):
+            return buf.at[pl.ds(first, blocks), pl.ds(pl.multiple_of(m * 2 * BLK, 2 * BLK), 2 * BLK), :]
+
+        def arrived_near(m):
+            ref = two(0, 3, m)
+            put(ref, ref, ss.at[2], near.at[m], (s, sib)).wait_recv()
+
+        def arrived_far(m):
+            ref = two(0, 1, m)
+            put(ref, ref, ss.at[2], far.at[m], (s, sib)).wait_recv()
+
+        def sent():
             for i in range(7):
-                hop(t, k, i, L1, right).wait_send()
-
-        return own, pass_on, pass_last, arrived, sent, arrived_near, arrived_opp
-
-    own, pass_on, pass_last, arrived, sent, arrived_near, arrived_opp = gather(X, BLK, xs_s, xs_r)
-    a_own, a_pass, a_last, a_arrived, a_sent, _, _ = gather(A, arows, as_s, as_r)
-    r_own, r_pass, r_last, r_arrived, r_sent, _, _ = gather(R, BLK, rs_s, rs_r)
+                put(buf.at[t], buf.at[t], ss.at[i], near.at[0], (s, sib)).wait_send()
+
+        return own, pass_on, pass_last, arrived_near, arrived_far, sent
+
+    own, pass_on, pass_last, arrived_near, arrived_far, sent = gather(X, BLK, xs_s, xs_r, xn_r, xf_r)
+    a_own, a_pass, a_last, a_near, a_far, a_sent = gather(A, arows, as_s, as_r, an_r, af_r)
+    r_own, r_pass, r_last, r_near, r_far, r_sent = gather(R, BLK, rs_s, rs_r, rn_r, rf_r)
 
     for k in range(AHEAD):
         own(k)
     for d in range(1, nx):
-        put(DX.at[x], DX.at[x], dx_s.at[d], dx_r.at[d], (z * nx + (x + d) % nx, t)).start()
+        put(DX.at[x], DX.at[x], dx_s.at[0], dx_r.at[0], (z * nx + (x + d) % nx, t)).start()
 
     lane_b = lax.broadcasted_iota(jnp.int32, (BLK, BLK), 1)
     row_b = lax.broadcasted_iota(jnp.int32, (BLK, BLK), 0)
@@ -185,16 +187,14 @@
         return acc, squares
 
     def project_near(m):
-        arrived_near(2 * m)
-        arrived_near(2 * m + 1)
+        arrived_near(m)
         zero = jnp.zeros((2 * BLK, 640), F32), jnp.zeros((2 * BLK, 128), F32)
-        ACC[m % 2], SQ[m % 2] = sums(m, *zero, (t, sib, left, right, sib_left, sib_right))
+        ACC[m], SQ[m] = sums(m, *zero, (t, sib, left, right, sib_left, sib_right))
 
     def project(m):
         two = pair(m)
-        arrived_opp(2 * m)
-        arrived_opp(2 * m + 1)
-        acc, squares = sums(m, ACC[m % 2], SQ[m % 2], (opp, sib_opp))
+        arrived_far(m)
+        acc, squares = sums(m, ACC[m], SQ[m], (opp, sib_opp))
         inv_rms = lax.rsqrt(jnp.sum(squares, axis=1, keepdims=True) / width + NORM_EPS)
         p = (acc * inv_rms).astype(BF16)
         Q[two, :] = p[:, 0:128]
@@ -257,12 +257,20 @@
             for d in range(1, 8):
                 to = (t + d) % 8
                 cols = pl.ds(pl.multiple_of(to * ocw, 128), ocw)
-                put(half.at[mine, cols], WO.at[i, t, mine, :], w1_s.at[i, d], w1_r.at[i, d], (s, to)).start()
+                put(half.at[mine, cols], WO.at[i, t, mine, :], w1_s.at[i], w1_r.at[i], (s, to)).start()
 
     def on(k):
         pass_on(k)
         if k + AHEAD < nb:
             own(k + AHEAD)
+
+    @pl.when(has_down == 0)
+    def _():
+        KV[0:BLK, :] = jnp.zeros((BLK, 128), BF16)
+
+    @pl.when(has_up == 0)
+    def _():
+        KV[rows + BLK : rows + 2 * BLK, :] = jnp.zeros((BLK, 128), BF16)
 
     on(0)
     on(1)
@@ -274,14 +282,18 @@
     pass_last(0)
     on(5)
     pass_last(1)
+    project_near(2)
     on(6)
     project(0)
-    halo_down.start()
+
+    @pl.when(has_down == 1)
+    def _():
+        halo_down.start()
+
     pass_last(2)
     on(7)
     weights_out()
     pass_last(3)
-    project_near(2)
     project(1)
     pass_last(4)
     pass_last(5)
@@ -290,11 +302,7 @@
     pass_last(6)
     project(2)
     pass_last(7)
-    attend(2)
-    attend(3)
-    a_own(1)
     project(3)
-    halo_up.start()
 
     f = jnp.zeros((64, RV), F32)
     g = jnp.zeros((64, RV), F32)
@@ -306,23 +314,33 @@
         g = jnp.exp(bl8[e : e + 1, :]) * g + TT[e, 64:128, :]
     XS[x, 0:64, :] = f.astype(BF16)
     XS[x, 64:128, :] = g.astype(BF16)
-    for d in range(1, nx):
-        put(XS.at[x], XS.at[x], sx_s.at[d], sx_r.at[d], (z * nx + (x + d) % nx, t)).start()
-
-    for d in range(1, nx):
-        o = (x + nx - d) % nx
-        put(DX.at[o], DX.at[o], dx_s.at[d], dx_r.at[d], (s, sib)).wait_recv()
+    for d in sorted(range(1, nx), key=lambda d: -min(d, nx - d)):
+        put(XS.at[x], XS.at[x], sx_s.at[0], sx_r.at[0], (z * nx + (x + d) % nx, t)).start()
+
+    @pl.when(has_up == 1)
+    def _():
+        halo_up.start()
+
+
+    put(DX.at[0 : nx - 1], DX.at[0 : nx - 1], dx_s.at[0], dx_r.at[0], (s, sib)).wait_recv()
     total = DX[0]
     for i in range(1, nx):
         total = total + DX[i]
     DZ[z] = total
     for d in range(1, nz):
-        put(DZ.at[z], DZ.at[z], dz_s.at[d], dz_r.at[d], (((z + d) % nz) * nx + x, t)).start()
-
+        put(DZ.at[z], DZ.at[z], dz_s.at[0], dz_r.at[0], (((z + d) % nz) * nx + x, t)).start()
+
+    attend(2)
+    attend(3)
+    a_own(1)
     attend(4)
     attend(5)
     a_own(2)
-    halo_down.wait_recv()
+
+    @pl.when(has_up == 1)
+    def _():
+        halo_down.wait_recv()
+
     attend(6)
     attend(7)
     a_own(3)
@@ -333,9 +351,8 @@
         return pl.ds(pl.multiple_of(((x + o + nx) % nx) * quarter, quarter), quarter)
 
     def w2_own(i):
-        for d in range(1, 8):
-            ref = WO.at[i, (t + 8 - d) % 8, mine, :]
-            put(ref, ref, w1_s.at[i, d], w1_r.at[i, d], (s, sib)).wait_recv()
+        ref = WO.at[i, 0:7, mine, :]
+        put(ref, ref, w1_s.at[i], w1_r.at[i], (s, sib)).wait_recv()
         ref = WO.at[i, :, mine, :]
         put(ref, ref, w2_s.at[i, 0], w2_r.at[i, 0], (xr, t)).start()
         put(ref, ref, w2_s.at[i, 1], w2_r.at[i, 1], (xl, t)).start()
@@ -364,33 +381,7 @@
         put(half, half, w2_s.at[i, 2], w2_r.at[i, 2], (xr, t)).wait_send()
         put(half, half, w2_s.at[i, 3], w2_r.at[i, 3], (xl, t)).wait_send()
 
-    w2_own(0)
-    w2_own(1)
-
-    def inside(j):
-        cc = column(j)
-        cr = crow[pl.ds(j, 1), :]
-        qk = QR[blk(j), :]
-        sc = lax.dot_general(qk[:, 0:64], qk[:, 64:128], NT, preferred_element_type=F32)
-        w = (sc * jnp.exp(-jnp.abs(cc - cr))).astype(BF16)
-        RL[blk(j), :] = jnp.dot(w, V[blk(j), :], preferred_element_type=F32) + jnp.dot(
-            QB[blk(j), :], SL[j], preferred_element_type=F32
-        )
-        gate = G[blk(j), :].astype(F32)
-        SG[blk(j), :] = gate / (1.0 + jnp.exp(-gate))
-
-    def inside_two(m, carry):
-        inside(2 * m)
-        inside(2 * m + 1)
-        return carry
-
-    lax.fori_loop(0, na, inside_two, 0)
-
-    a_pass(1)
-
-    for d in range(1, nx):
-        o = (x + nx - d) % nx
-        put(XS.at[o], XS.at[o], sx_s.at[d], sx_r.at[d], (s, sib)).wait_recv()
+    put(XS.at[0 : nx - 1], XS.at[0 : nx - 1], sx_s.at[0], sx_r.at[0], (s, sib)).wait_recv()
     ex = [jnp.exp(DX[i][0:1, :]) for i in range(nx)]
     fx = jnp.zeros((64, RV), F32)
     gx = jnp.zeros((64, RV), F32)
@@ -411,29 +402,58 @@
     ZG[0] = fall.astype(BF16)
     ZG[1] = gall.astype(BF16)
     ZS[z] = jnp.zeros((64, RV), BF16)
-    for d in range(1, nz):
-        put(ZG.at[(z + d) // nz], ZS.at[z], sz_s.at[d], sz_r.at[d], (((z + d) % nz) * nx + x, t)).start()
-
-    halo_up.wait_recv()
+    for d in sorted(range(1, nz), key=lambda d: -min(d, nz - d)):
+        put(ZG.at[(z + d) // nz], ZS.at[z], sz_s.at[0], sz_r.at[0], (((z + d) % nz) * nx + x, t)).start()
+
+    w2_own(0)
+    w2_own(1)
+
+    @pl.when(has_down == 1)
+    def _():
+        halo_up.wait_recv()
+
     attend(0)
     a_own(0)
 
-    for k in range(2, na):
-        a_pass(k)
-
-    def drain(k, carry):
-        sent(k)
+    def inside(j):
+        cc = column(j)
+        cr = crow[pl.ds(j, 1), :]
+        qk = QR[blk(j), :]
+        sc = lax.dot_general(qk[:, 0:64], qk[:, 64:128], NT, preferred_element_type=F32)
+        w = (sc * jnp.exp(-jnp.abs(cc - cr))).astype(BF16)
+        RL[blk(j), :] = jnp.dot(w, V[blk(j), :], preferred_element_type=F32) + jnp.dot(
+            QB[blk(j), :], SL[j], preferred_element_type=F32
+        )
+        gate = G[blk(j), :].astype(F32)
+        SG[blk(j), :] = gate / (1.0 + jnp.exp(-gate))
+
+    def inside_two(m, carry):
+        inside(2 * m)
+        inside(2 * m + 1)
         return carry
 
-    lax.fori_loop(0, nb, drain, 0)
+
+    a_pass(1)
+    lax.fori_loop(0, na // 2, inside_two, 0)
+    a_pass(2)
+    lax.fori_loop(na // 2, na, inside_two, 0)
+    a_pass(3)
+
+    sent()
     for i in range(2):
-        for d in range(1, 8):
-            put(oa_h.at[mine, my_cols], WO.at[i, t, mine, :], w1_s.at[i, d], w1_r.at[i, d], (s, sib)).wait_send()
-    for d in range(1, nx):
-        put(XS.at[x], XS.at[x], sx_s.at[d], sx_r.at[d], (s, sib)).wait_send()
-        put(DX.at[x], DX.at[x], dx_s.at[d], dx_r.at[d], (s, sib)).wait_send()
-    halo_up.wait_send()
-    halo_down.wait_send()
+        ref = WO.at[i, 0:7, mine, :]
+        put(ref, ref, w1_s.at[i], w1_r.at[i], (s, sib)).wait_send()
+    put(XS.at[0 : nx - 1], XS.at[0 : nx - 1], sx_s.at[0], sx_r.at[0], (s, sib)).wait_send()
+    put(DX.at[0 : nx - 1], DX.at[0 : nx - 1], dx_s.at[0], dx_r.at[0], (s, sib)).wait_send()
+
+    @pl.when(has_up == 1)
+    def _():
+        halo_up.wait_send()
+
+    @pl.when(has_down == 1)
+    def _():
+        halo_down.wait_send()
+
 
     a_last(1)
     w2_pass(0)
@@ -442,10 +462,9 @@
     a_pass(0)
     w2_pass(1)
 
-    for d in range(1, nz):
-        o = (z + nz - d) % nz
-        put(DZ.at[o], DZ.at[o], dz_s.at[d], dz_r.at[d], (s, sib)).wait_recv()
-        put(ZS.at[o], ZS.at[o], sz_s.at[d], sz_r.at[d], (s, sib)).wait_recv()
+    if nz > 1:
+        put(DZ.at[0 : nz - 1], DZ.at[0 : nz - 1], dz_s.at[0], dz_r.at[0], (s, sib)).wait_recv()
+        put(ZS.at[0 : nz - 1], ZS.at[0 : nz - 1], sz_s.at[0], sz_r.at[0], (s, sib)).wait_recv()
     fz = init[0:64, :]
     gz = init[64:128, :]
     for i in range(nz):
@@ -475,33 +494,35 @@
         OA[big(k), :] = jnp.dot(lhs, WO[0].reshape(8 * BLK, ocw), preferred_element_type=F32)
 
     def out_ret(k):
-        r_arrived(2 * k)
-        r_arrived(2 * k + 1)
+        r_near(k)
+        r_far(k)
         lhs = jnp.concatenate([R[b, big(k), :] for b in range(8)], axis=1)
         acc = OA[big(k), :] + jnp.dot(lhs, WO[1].reshape(8 * BLK, ocw), preferred_element_type=F32)
         OUT[big(k), :] = acc.astype(BF16)
         pltpu.make_async_copy(OUT.at[big(k), :], out_h.at[big(k), :], lsem.at[14 + k]).start()
 
-    w2_done(0)
-    for k in range(1, na):
-        a_arrived(k)
-        out_att(k)
     for k in range(nb):
         r_pass(k)
         if k == 1:
             a_last(0)
-    a_arrived(0)
+        if k == nb // 2 - 1:
+            w2_done(0)
+        if nb // 2 <= k < nb - 1:
+            a_near(k - nb // 2 + 1)
+            a_far(k - nb // 2 + 1)
+            out_att(k - nb // 2 + 1)
+    a_near(0)
+    a_far(0)
     out_att(0)
     for k in range(nb // 2):
         r_last(k)
     w2_done(1)
-    for k in range(na):
-        a_sent(k)
+    a_sent()
     for i in range(2):
         w2_sent(i)
-    for d in range(1, nz):
-        put(ZG.at[0], ZS.at[z], sz_s.at[d], sz_r.at[d], (s, sib)).wait_send()
-        put(DZ.at[z], DZ.at[z], dz_s.at[d], dz_r.at[d], (s, sib)).wait_send()
+    if nz > 1:
+        put(ZS.at[0 : nz - 1], ZS.at[0 : nz - 1], sz_s.at[0], sz_r.at[0], (s, sib)).wait_send()
+        put(DZ.at[0 : nz - 1], DZ.at[0 : nz - 1], dz_s.at[0], dz_r.at[0], (s, sib)).wait_send()
     out_ret(0)
     r_last(4)
     r_last(5)
@@ -509,12 +530,9 @@
     r_last(6)
     r_last(7)
     out_ret(2)
-    for k in range(nb // 2):
-        r_sent(k)
     out_ret(3)
 
-    for k in range(nb // 2, nb):
-        r_sent(k)
+    r_sent()
     for k in range(na):
         pltpu.make_async_copy(OUT.at[big(k), :], out_h.at[big(k), :], lsem.at[14 + k]).wait()
 
@@ -537,14 +555,15 @@
         vm((8, rows, cw), BF16), vm((width, 640), BF16), vm((256, width), BF16), vm((1, width), F32), vm((1, rows), F32),
         vm((128, 128), F32), vm((1, 128), F32),
         vm((rows, 128), BF16), vm((rows + 2 * BLK, 128), BF16), vm((rows, 128), BF16), vm((rows, 128), BF16), vm((rows, 128), F32),
-        vm((rows, 128), F32), vm((rows, 128), F32), vm((2, 2 * BLK, 640), F32), vm((2, 2 * BLK, 128), F32), vm((rows, 128), BF16), vm((rows, 128), BF16), vm((rows, 128), BF16), vm((rows, 128), F32),
+        vm((rows, 128), F32), vm((rows, 128), F32), vm((nb // 2, 2 * BLK, 640), F32), vm((nb // 2, 2 * BLK, 128), F32), vm((rows, 128), BF16), vm((rows, 128), BF16), vm((rows, 128), BF16), vm((rows, 128), F32),
         vm((nb, 128, 128), F32), vm((nb, 128, 128), BF16),
         vm((8, rows, 128), BF16), vm((8, rows, 128), BF16), vm((2, 8, 128, ocw), BF16), vm((rows, ocw), F32), vm((rows, ocw), BF16),
         vm((nx, 128, 128), BF16), vm((2, 64, 128), BF16), vm((nz, 64, 128), BF16), vm((nx, 8, 128), F32), vm((nz, 8, 128), F32),
         vm((nb, 128), F32), vm((nb, 128), F32), vm((nb, 128), F32),
-        dma((14 + nb,)), dma((7, nb)), dma((7, nb)), dma((7, na)), dma((7, na)), dma((7, nb)), dma((7, nb)),
-        dma((2, 8)), dma((2, 8)), dma((2, 4)), dma((2, 4)), dma((nx,)), dma((nx,)), dma((nx,)), dma((nx,)),
-        dma((max(nz, 2),)), dma((max(nz, 2),)), dma((max(nz, 2),)), dma((max(nz, 2),)), dma((2,)), dma((2,)),
+        dma((14 + na,)), dma((7,)), dma((3, nb)), dma((na,)), dma((na,)), dma((7,)), dma((3, na)), dma((na,)), dma((na,)),
+        dma((7,)), dma((3, nb)), dma((na,)), dma((na,)),
+        dma((2,)), dma((2,)), dma((2, 4)), dma((2, 4)), dma((1,)), dma((1,)), dma((1,)), dma((1,)),
+        dma((1,)), dma((1,)), dma((1,)), dma((1,)), dma((2,)), dma((2,)),
     ]
     call = pl.pallas_call(
         functools.partial(kernel, n_sp, nx),

time: 65.6 us -> 63.1 us (0.962)
  Pallas kernels: 63.6 us -> 61.1 us
    pallas_call x1, Pallas kernels: 63.6 us -> 61.1 us  [body(): call(tokens, norm_gain.reshape(1, width), att_query, att_key.T, att_value...]
where the time goes in v5:
time: 63.1 us; the launch traced here: 63 us
  Pallas kernels  61.1 us (97%)
  local copies, waits for them, and re-layouts  1.87 us (3%)
    pallas_call x1, Pallas kernels, body(): call(tokens, norm_gain.reshape(1, width), att_query, att_key.T, att_value...  61.1 us
    unnamed x1, local copies, waits for them, and re-layouts  1.87 us

profile of v5, /device:TPU:1, one launch (start us, length us, event | category | flops | bytes accessed | tf_op | source)
XLA Modules:
  0.0 63.0 jit_solution(14912615557418080969)
XLA Ops:
  0.0 61.1 %layer.1 = bf16[1024,256]{1,0:T(8,128)(2,1)} custom-call(bf16[1024,256]{1,0:T(8,128)(2,1)} %tok_h.1, f32[1,2048]{1,0:T(1,128)} %bitcast.11, bf16[2048,128]{1,0:T(8,128)(2,1)} %wq_h.1, bf16[64,2048]{1,0:T(8,128)(2,1)} %bitcast.6, bf16[64,2048]{1,0:T(8,128)(2,1)} %bitcast.7, bf16[64,2048]{1,0:T(8,128)(2,1)} %bitcast.8, bf16[64,2048]{1,0:T(8,128)(2,1)} %bitcast.9, ...), custom_call_target="tpu_custom_call" | custom-call | tf_op jit(solution)/shard_map/layer/pallas_call | solution.py:577
  61.1 1.9 %copy.17 = bf16[1024,256]{1,0:T(8,128)(2,1)} copy(bf16[1024,256]{1,0:T(8,128)(2,1)} %layer.1) | data formatting | bytes 1048576

commit v6 on v5

--- a/solution.py
+++ b/solution.py
@@ -106,43 +106,42 @@
         def part(b, k):
             return buf.at[b, pl.ds(pl.multiple_of(k * n_rows, n_rows), n_rows), :]
 
-        def hop(b, k, send, recv, tp):
+        def hop(b, k, recv, tp):
             ref = part(b, k)
-            return put(ref, ref, ss.at[send], recv, (s, tp))
+            return put(ref, ref, ss.at[0], recv, (s, tp))
 
         def own(k):
-            hop(t, k, 0, rs.at[L1, k], right).start()
-            hop(t, k, 1, rs.at[R1, k], left).start()
-            hop(t, k, 2, near.at[k // group], sib).start()
+            hop(t, k, rs.at[L1, k], right).start()
+            hop(t, k, rs.at[R1, k], left).start()
+            hop(t, k, near.at[k // group], sib).start()
 
         def pass_on(k):
-            hop(left, k, 3, rs.at[L1, k], right).wait_recv()
+            hop(left, k, rs.at[L1, k], right).wait_recv()
             if k % 2 == 0:
-                hop(left, k, 6, rs.at[OPP, k], right).start()
-            hop(left, k, 3, near.at[k // group], sib).start()
-            hop(right, k, 4, rs.at[R1, k], left).wait_recv()
+                hop(left, k, rs.at[OPP, k], right).start()
+            hop(left, k, near.at[k // group], sib).start()
+            hop(right, k, rs.at[R1, k], left).wait_recv()
             if k % 2 == 1:
-                hop(right, k, 6, rs.at[OPP, k], left).start()
-            hop(right, k, 4, near.at[k // group], sib).start()
+                hop(right, k, rs.at[OPP, k], left).start()
+            hop(right, k, near.at[k // group], sib).start()
 
         def pass_last(k):
-            hop(opp, k, 5, rs.at[OPP, k], right).wait_recv()
-            hop(opp, k, 5, far.at[k // group], sib).start()
+            hop(opp, k, rs.at[OPP, k], right).wait_recv()
+            hop(opp, k, far.at[k // group], sib).start()
 
         def two(first, blocks, m):
             return buf.at[pl.ds(first, blocks), pl.ds(pl.multiple_of(m * 2 * BLK, 2 * BLK), 2 * BLK), :]
 
         def arrived_near(m):
             ref = two(0, 3, m)
-            put(ref, ref, ss.at[2], near.at[m], (s, sib)).wait_recv()
+            put(ref, ref, ss.at[0], near.at[m], (s, sib)).wait_recv()
 
         def arrived_far(m):
             ref = two(0, 1, m)
-            put(ref, ref, ss.at[2], far.at[m], (s, sib)).wait_recv()
+            put(ref, ref, ss.at[0], far.at[m], (s, sib)).wait_recv()
 
         def sent():
-            for i in range(7):
-                put(buf.at[t], buf.at[t], ss.at[i], near.at[0], (s, sib)).wait_send()
+            put(buf.at[0:7], buf.at[0:7], ss.at[0], near.at[0], (s, sib)).wait_send()
 
         return own, pass_on, pass_last, arrived_near, arrived_far, sent
 
@@ -282,27 +281,49 @@
     pass_last(0)
     on(5)
     pass_last(1)
-    project_near(2)
-    on(6)
-    project(0)
-
-    @pl.when(has_down == 1)
-    def _():
-        halo_down.start()
-
-    pass_last(2)
-    on(7)
-    weights_out()
-    pass_last(3)
-    project(1)
-    pass_last(4)
-    pass_last(5)
-    project_near(3)
-    attend(1)
-    pass_last(6)
-    project(2)
-    pass_last(7)
-    project(3)
+
+    def keys_down():
+        @pl.when(has_down == 1)
+        def _():
+            halo_down.start()
+
+    @pl.when(c == 0)
+    def _():
+        project_near(2)
+        on(6)
+        project(0)
+        keys_down()
+        pass_last(2)
+        on(7)
+        weights_out()
+        pass_last(3)
+        project(1)
+        project_near(3)
+        pass_last(4)
+        pass_last(5)
+        project(2)
+        pass_last(6)
+        pass_last(7)
+        project(3)
+
+    @pl.when(c == 1)
+    def _():
+        on(6)
+        pass_last(2)
+        on(7)
+        weights_out()
+        project_near(2)
+        project(0)
+        keys_down()
+        pass_last(3)
+        pass_last(4)
+        pass_last(5)
+        project(1)
+        pass_last(6)
+        project_near(3)
+        pass_last(7)
+        project(2)
+        project(3)
 
     f = jnp.zeros((64, RV), F32)
     g = jnp.zeros((64, RV), F32)
@@ -330,6 +351,7 @@
     for d in range(1, nz):
         put(DZ.at[z], DZ.at[z], dz_s.at[0], dz_r.at[0], (((z + d) % nz) * nx + x, t)).start()
 
+    attend(1)
     attend(2)
     attend(3)
     a_own(1)
@@ -354,32 +376,28 @@
         ref = WO.at[i, 0:7, mine, :]
         put(ref, ref, w1_s.at[i], w1_r.at[i], (s, sib)).wait_recv()
         ref = WO.at[i, :, mine, :]
-        put(ref, ref, w2_s.at[i, 0], w2_r.at[i, 0], (xr, t)).start()
-        put(ref, ref, w2_s.at[i, 1], w2_r.at[i, 1], (xl, t)).start()
+        put(ref, ref, w2_s.at[i], w2_r.at[i, 0], (xr, t)).start()
+        put(ref, ref, w2_s.at[i], w2_r.at[i, 1], (xl, t)).start()
 
     def w2_pass(i):
         from_left = WO.at[i, :, quarter_of(-1), :]
         from_right = WO.at[i, :, quarter_of(1), :]
-        put(from_left, from_left, w2_s.at[i, 0], w2_r.at[i, 0], (xr, t)).wait_recv()
+        put(from_left, from_left, w2_s.at[i], w2_r.at[i, 0], (xr, t)).wait_recv()
         half = WO.at[i, 0:4, quarter_of(-1), :]
-        put(half, half, w2_s.at[i, 2], w2_r.at[i, 2], (xr, t)).start()
-        put(from_right, from_right, w2_s.at[i, 1], w2_r.at[i, 1], (xl, t)).wait_recv()
+        put(half, half, w2_s.at[i], w2_r.at[i, 2], (xr, t)).start()
+        put(from_right, from_right, w2_s.at[i], w2_r.at[i, 1], (xl, t)).wait_recv()
         half = WO.at[i, 4:8, quarter_of(1), :]
-        put(half, half, w2_s.at[i, 3], w2_r.at[i, 3], (xl, t)).start()
+        put(half, half, w2_s.at[i], w2_r.at[i, 3], (xl, t)).start()
 
     def w2_done(i):
         half = WO.at[i, 0:4, quarter_of(2), :]
-        put(half, half, w2_s.at[i, 2], w2_r.at[i, 2], (xr, t)).wait_recv()
+        put(half, half, w2_s.at[i], w2_r.at[i, 2], (xr, t)).wait_recv()
         half = WO.at[i, 4:8, quarter_of(2), :]
-        put(half, half, w2_s.at[i, 3], w2_r.at[i, 3], (xl, t)).wait_recv()
+        put(half, half, w2_s.at[i], w2_r.at[i, 3], (xl, t)).wait_recv()
 
     def w2_sent(i):
-        ref = WO.at[i, :, mine, :]
-        half = WO.at[i, 0:4, mine, :]
-        put(ref, ref, w2_s.at[i, 0], w2_r.at[i, 0], (xr, t)).wait_send()
-        put(ref, ref, w2_s.at[i, 1], w2_r.at[i, 1], (xl, t)).wait_send()
-        put(half, half, w2_s.at[i, 2], w2_r.at[i, 2], (xr, t)).wait_send()
-        put(half, half, w2_s.at[i, 3], w2_r.at[i, 3], (xl, t)).wait_send()
+        ref = WO.at[i, :, 0 : 3 * quarter, :]
+        put(ref, ref, w2_s.at[i], w2_r.at[i, 0], (xr, t)).wait_send()
 
     put(XS.at[0 : nx - 1], XS.at[0 : nx - 1], sx_s.at[0], sx_r.at[0], (s, sib)).wait_recv()
     ex = [jnp.exp(DX[i][0:1, :]) for i in range(nx)]
@@ -455,12 +473,7 @@
         halo_down.wait_send()
 
 
-    a_last(1)
-    w2_pass(0)
-    a_last(2)
-    a_last(3)
     a_pass(0)
-    w2_pass(1)
 
     if nz > 1:
         put(DZ.at[0 : nz - 1], DZ.at[0 : nz - 1], dz_s.at[0], dz_r.at[0], (s, sib)).wait_recv()
@@ -502,9 +515,13 @@
         pltpu.make_async_copy(OUT.at[big(k), :], out_h.at[big(k), :], lsem.at[14 + k]).start()
 
     for k in range(nb):
+        if k == 0:
+            for i in range(1, na):
+                a_last(i)
+            w2_pass(0)
+            a_last(0)
+            w2_pass(1)
         r_pass(k)
-        if k == 1:
-            a_last(0)
         if k == nb // 2 - 1:
             w2_done(0)
         if nb // 2 <= k < nb - 1:
@@ -560,9 +577,9 @@
         vm((8, rows, 128), BF16), vm((8, rows, 128), BF16), vm((2, 8, 128, ocw), BF16), vm((rows, ocw), F32), vm((rows, ocw), BF16),
         vm((nx, 128, 128), BF16), vm((2, 64, 128), BF16), vm((nz, 64, 128), BF16), vm((nx, 8, 128), F32), vm((nz, 8, 128), F32),
         vm((nb, 128), F32), vm((nb, 128), F32), vm((nb, 128), F32),
-        dma((14 + na,)), dma((7,)), dma((3, nb)), dma((na,)), dma((na,)), dma((7,)), dma((3, na)), dma((na,)), dma((na,)),
-        dma((7,)), dma((3, nb)), dma((na,)), dma((na,)),
-        dma((2,)), dma((2,)), dma((2, 4)), dma((2, 4)), dma((1,)), dma((1,)), dma((1,)), dma((1,)),
+        dma((14 + na,)), dma((1,)), dma((3, nb)), dma((na,)), dma((na,)), dma((1,)), dma((3, na)), dma((na,)), dma((na,)),
+        dma((1,)), dma((3, nb)), dma((na,)), dma((na,)),
+        dma((2,)), dma((2,)), dma((2,)), dma((2, 4)), dma((1,)), dma((1,)), dma((1,)), dma((1,)),
         dma((1,)), dma((1,)), dma((1,)), dma((1,)), dma((2,)), dma((2,)),
     ]
     call = pl.pallas_call(

time: 63.1 us -> 60.9 us (0.965)
  Pallas kernels: 61.1 us -> 58.9 us
    pallas_call x1, Pallas kernels: 61.1 us -> 58.9 us  [body(): call(tokens, norm_gain.reshape(1, width), att_query, att_key.T, att_value...]
where the time goes in v6:
time: 60.9 us; the launch traced here: 60.8 us
  Pallas kernels  58.9 us (97%)
  local copies, waits for them, and re-layouts  1.87 us (3%)
    pallas_call x1, Pallas kernels, body(): call(tokens, norm_gain.reshape(1, width), att_query, att_key.T, att_value...  58.9 us
    unnamed x1, local copies, waits for them, and re-layouts  1.87 us

profile of v6, /device:TPU:1, one launch (start us, length us, event | category | flops | bytes accessed | tf_op | source)
XLA Modules:
  0.0 60.8 jit_solution(11014887486237150092)
XLA Ops:
  0.0 58.9 %layer.1 = bf16[1024,256]{1,0:T(8,128)(2,1)} custom-call(bf16[1024,256]{1,0:T(8,128)(2,1)} %tok_h.1, f32[1,2048]{1,0:T(1,128)} %bitcast.11, bf16[2048,128]{1,0:T(8,128)(2,1)} %wq_h.1, bf16[64,2048]{1,0:T(8,128)(2,1)} %bitcast.6, bf16[64,2048]{1,0:T(8,128)(2,1)} %bitcast.7, bf16[64,2048]{1,0:T(8,128)(2,1)} %bitcast.8, bf16[64,2048]{1,0:T(8,128)(2,1)} %bitcast.9, ...), custom_call_target="tpu_custom_call" | custom-call | tf_op jit(solution)/shard_map/layer/pallas_call | solution.py:594
  58.9 1.9 %copy.17 = bf16[1024,256]{1,0:T(8,128)(2,1)} copy(bf16[1024,256]{1,0:T(8,128)(2,1)} %layer.1) | data formatting | bytes 1048576

commit v7 on v6

--- a/solution.py
+++ b/solution.py
@@ -24,8 +24,8 @@
 
 
 def kernel(n_sp, nx, tok_h, gain_h, wq_h, wk_h, wv_h, wrq_h, wrk_h, wrv_h, wrg_h, sink_ref, dec_h, init_h, inv_h, oa_h, or_h,
-           out_h,
-           X, W1, W2, gain, dec, init, inv, Q, KV, V, G, SG, COS, SIN, ACC, SQ, QR, QB, QX, RL, TT, SL, A, R, WO, OA, OUT,
+           OUT,
+           X, W1, W2, gain, dec, init, inv, Q, KV, V, G, SG, COS, SIN, ACC, SQ, QR, QB, QX, RL, TT, SL, A, R, WO, OA,
            XS, ZG, ZS, DX, DZ, crow, bl8, pre8,
            lsem, xs_s, xs_r, xn_r, xf_r, as_s, as_r, an_r, af_r, rs_s, rs_r, rn_r, rf_r, w1_s, w1_r, w2_s, w2_r, sx_s, sx_r, dx_s, dx_r, sz_s, sz_r, dz_s, dz_r,
            h_s, h_r):
@@ -512,7 +512,6 @@
         lhs = jnp.concatenate([R[b, big(k), :] for b in range(8)], axis=1)
         acc = OA[big(k), :] + jnp.dot(lhs, WO[1].reshape(8 * BLK, ocw), preferred_element_type=F32)
         OUT[big(k), :] = acc.astype(BF16)
-        pltpu.make_async_copy(OUT.at[big(k), :], out_h.at[big(k), :], lsem.at[14 + k]).start()
 
     for k in range(nb):
         if k == 0:
@@ -550,8 +549,6 @@
     out_ret(3)
 
     r_sent()
-    for k in range(na):
-        pltpu.make_async_copy(OUT.at[big(k), :], out_h.at[big(k), :], lsem.at[14 + k]).wait()
 
 
 def body(tokens, norm_gain, att_query, att_key, att_value, ret_query, ret_key, ret_value, ret_gate, att_sink, decay_log, init_state,
@@ -574,21 +571,21 @@
         vm((rows, 128), BF16), vm((rows + 2 * BLK, 128), BF16), vm((rows, 128), BF16), vm((rows, 128), BF16), vm((rows, 128), F32),
         vm((rows, 128), F32), vm((rows, 128), F32), vm((nb // 2, 2 * BLK, 640), F32), vm((nb // 2, 2 * BLK, 128), F32), vm((rows, 128), BF16), vm((rows, 128), BF16), vm((rows, 128), BF16), vm((rows, 128), F32),
         vm((nb, 128, 128), F32), vm((nb, 128, 128), BF16),
-        vm((8, rows, 128), BF16), vm((8, rows, 128), BF16), vm((2, 8, 128, ocw), BF16), vm((rows, ocw), F32), vm((rows, ocw), BF16),
+        vm((8, rows, 128), BF16), vm((8, rows, 128), BF16), vm((2, 8, 128, ocw), BF16), vm((rows, ocw), F32),
         vm((nx, 128, 128), BF16), vm((2, 64, 128), BF16), vm((nz, 64, 128), BF16), vm((nx, 8, 128), F32), vm((nz, 8, 128), F32),
         vm((nb, 128), F32), vm((nb, 128), F32), vm((nb, 128), F32),
-        dma((14 + na,)), dma((1,)), dma((3, nb)), dma((na,)), dma((na,)), dma((1,)), dma((3, na)), dma((na,)), dma((na,)),
+        dma((14,)), dma((1,)), dma((3, nb)), dma((na,)), dma((na,)), dma((1,)), dma((3, na)), dma((na,)), dma((na,)),
         dma((1,)), dma((3, nb)), dma((na,)), dma((na,)),
         dma((2,)), dma((2,)), dma((2,)), dma((2, 4)), dma((1,)), dma((1,)), dma((1,)), dma((1,)),
         dma((1,)), dma((1,)), dma((1,)), dma((1,)), dma((2,)), dma((2,)),
     ]
     call = pl.pallas_call(
         functools.partial(kernel, n_sp, nx),
-        out_shape=jax.ShapeDtypeStruct((rows, ocw), BF16),
+        out_shape=pltpu.VMEM((rows, ocw), BF16),
         in_specs=specs,
-        out_specs=hbm,
+        out_specs=pl.BlockSpec(memory_space=pltpu.VMEM),
         scratch_shapes=scratch,
-        compiler_params=pltpu.CompilerParams(collective_id=0, has_side_effects=True, vmem_limit_bytes=67_043_328),
+        compiler_params=pltpu.CompilerParams(collective_id=0, has_side_effects=True, vmem_limit_bytes=66_000_000),
         name="layer",
     )
     return call(

time: 60.9 us -> 59.1 us (0.970)
  local copies, waits for them, and re-layouts: 1.87 us -> 0.8 us
  Pallas kernels: 58.9 us -> 58.2 us
    unnamed x1, local copies, waits for them, and re-layouts: 1.87 us -> 0.8 us
    pallas_call x1, Pallas kernels: 58.9 us -> 58.2 us  [body(): call(tokens, norm_gain.reshape(1, width), att_query, att_key.T, att_value...]
where the time goes in v7:
time: 59.1 us; the launch traced here: 59 us
  Pallas kernels  58.2 us (98%)
  local copies, waits for them, and re-layouts  0.8 us (1%)
    pallas_call x1, Pallas kernels, body(): call(tokens, norm_gain.reshape(1, width), att_query, att_key.T, att_value...  58.2 us

profile of v7, /device:TPU:1, one launch (start us, length us, event | category | flops | bytes accessed | tf_op | source)
XLA Modules:
  0.0 59.0 jit_solution(447696214671824875)
XLA Ops:
  0.0 58.2 %layer.1 = bf16[1024,256]{1,0:T(8,128)(2,1)S(1)} custom-call(bf16[1024,256]{1,0:T(8,128)(2,1)} %tok_h.1, f32[1,2048]{1,0:T(1,128)} %bitcast.11, bf16[2048,128]{1,0:T(8,128)(2,1)} %wq_h.1, bf16[64,2048]{1,0:T(8,128)(2,1)} %bitcast.6, bf16[64,2048]{1,0:T(8,128)(2,1)} %bitcast.7, bf16[64,2048]{1,0:T(8,128)(2,1)} %bitcast.8, bf16[64,2048]{1,0:T(8,128)(2,1)} %bitcast.9, ...), custom_call_target="tpu_custom_call" | custom-call | tf_op jit(solution)/shard_map/layer/pallas_call | solution.py:591
  58.2 0.8 %copy.17 = bf16[1024,256]{1,0:T(8,128)(2,1)} copy(bf16[1024,256]{1,0:T(8,128)(2,1)S(1)} %layer.1) | data formatting | bytes 1048576

commit v8 on v7

--- a/solution.py
+++ b/solution.py
@@ -506,12 +506,18 @@
         lhs = jnp.concatenate([A[b, big(k), :] for b in range(8)], axis=1)
         OA[big(k), :] = jnp.dot(lhs, WO[0].reshape(8 * BLK, ocw), preferred_element_type=F32)
 
+    def ret_sum(k, blocks):
+        lhs = jnp.concatenate([R[b, big(k), :] for b in blocks], axis=1)
+        rhs = jnp.concatenate([WO[1, b] for b in blocks], axis=0)
+        return OA[big(k), :] + jnp.dot(lhs, rhs, preferred_element_type=F32)
+
+    def out_near(k):
+        r_near(k)
+        OA[big(k), :] = ret_sum(k, (t, sib, left, right, sib_left, sib_right))
+
     def out_ret(k):
-        r_near(k)
         r_far(k)
-        lhs = jnp.concatenate([R[b, big(k), :] for b in range(8)], axis=1)
-        acc = OA[big(k), :] + jnp.dot(lhs, WO[1].reshape(8 * BLK, ocw), preferred_element_type=F32)
-        OUT[big(k), :] = acc.astype(BF16)
+        OUT[big(k), :] = ret_sum(k, (opp, sib_opp)).astype(BF16)
 
     for k in range(nb):
         if k == 0:
@@ -539,14 +545,16 @@
     if nz > 1:
         put(ZS.at[0 : nz - 1], ZS.at[0 : nz - 1], sz_s.at[0], sz_r.at[0], (s, sib)).wait_send()
         put(DZ.at[0 : nz - 1], DZ.at[0 : nz - 1], dz_s.at[0], dz_r.at[0], (s, sib)).wait_send()
-    out_ret(0)
+    out_near(0)
+    out_near(1)
     r_last(4)
     r_last(5)
-    out_ret(1)
+    out_near(2)
+    out_near(3)
     r_last(6)
     r_last(7)
-    out_ret(2)
-    out_ret(3)
+    for k in range(na):
+        out_ret(k)
 
     r_sent()
 

time: 59.1 us -> 58.9 us (level)
  no operation moved by 1% of the time
where the time goes in v8:
time: 58.9 us; the launch traced here: 58.8 us
  Pallas kernels  58 us (98%)
  local copies, waits for them, and re-layouts  0.8 us (1%)
    pallas_call x1, Pallas kernels, body(): call(tokens, norm_gain.reshape(1, width), att_query, att_key.T, att_value...  58 us

profile of v8, /device:TPU:1, one launch (start us, length us, event | category | flops | bytes accessed | tf_op | source)
XLA Modules:
  0.0 58.8 jit_solution(11320358317272014866)
XLA Ops:
  0.0 58.0 %layer.1 = bf16[1024,256]{1,0:T(8,128)(2,1)S(1)} custom-call(bf16[1024,256]{1,0:T(8,128)(2,1)} %tok_h.1, f32[1,2048]{1,0:T(1,128)} %bitcast.11, bf16[2048,128]{1,0:T(8,128)(2,1)} %wq_h.1, bf16[64,2048]{1,0:T(8,128)(2,1)} %bitcast.6, bf16[64,2048]{1,0:T(8,128)(2,1)} %bitcast.7, bf16[64,2048]{1,0:T(8,128)(2,1)} %bitcast.8, bf16[64,2048]{1,0:T(8,128)(2,1)} %bitcast.9, ...), custom_call_target="tpu_custom_call" | custom-call | tf_op jit(solution)/shard_map/layer/pallas_call | solution.py:599
  58.0 0.8 %copy.17 = bf16[1024,256]{1,0:T(8,128)(2,1)} copy(bf16[1024,256]{1,0:T(8,128)(2,1)S(1)} %layer.1) | data formatting | bytes 1048576
